TPU v7x, 512 devices: a whole 4x4x16 slice. The times are simulated.
512 devices in a mesh: sp: 64 (over z, y), tp: 8 (over x, core).
Axes of the slice: x: 4, y: 4, z: 16, core: 2. Of those that a mesh axis runs over, the one named last changes fastest.
Arguments:
- mixer_in: bfloat16 [32768, 1024], P('sp', 'tp'), may hold values from -6 to 6
- residual: bfloat16 [32768, 2048], P(('sp', 'tp')), may hold values from -6 to 6
- decay_real: float32 [64, 64], P('tp'), may hold values from -2 to 0, as said below
- decay_imag: float32 [64, 64], P('tp'), may hold values from 1 to 200
- log_step: float32 [64], P('tp'), may hold values from -3.9 to -2.5
- in_real: float32 [64, 64, 16], P('tp'), may hold values from -1 to 1
- in_imag: float32 [64, 64, 16], P('tp'), may hold values from -1 to 1
- output_real: float32 [64, 16, 64], P('tp'), may hold values from -0.5 to 0.5
- output_imaginary: float32 [64, 16, 64], P('tp'), may hold values from -0.5 to 0.5
- skip: float32 [1024], P('tp'), may hold values from -4 to 4
- out_proj: bfloat16 [1024, 2048], P('tp'), may hold values from -0.1875 to 0.1875
- norm_gain: float32 [2048], replicated, may hold values from 0.1 to 1.9
- w_gate: bfloat16 [2048, 5632], P('sp', 'tp'), may hold values from -0.125 to 0.125
- w_up: bfloat16 [2048, 5632], P('sp', 'tp'), may hold values from -0.125 to 0.125
- w_down: bfloat16 [5632, 2048], P('tp', 'sp'), may hold values from -0.078125 to 0.078125
Outputs:
- output: bfloat16 [32768, 2048], P(('sp', 'tp'))
Inputs may be any that keep to these rules, and one draw needn't show every extreme that they name: `decay_real`: every entry is negative.
All inputs are finite; a program needn't handle non-finite values.
Results may differ from a plain program's by a relative error of at most 0.02.
Values may be sent and summed in bfloat16 or wider, within the bound.
A program may use at most 64 MiB of HBM per device.

v0:
```python
import jax
import jax.numpy as jnp
from jax import lax
from jax.sharding import Mesh
from jax.sharding import PartitionSpec as P

SP = ("sp_0", "sp_1")
SP_TP = ("sp_0", "sp_1", "tp")


def side_by_side(arrays, axis, dim, along):
    widths = [a.shape[along] for a in arrays]
    both = jnp.concatenate(arrays, axis=along)
    result = lax.all_gather(both, axis, axis=dim, tiled=True)
    return tuple(jnp.split(result, [sum(widths[:k]) for k in range(1, len(widths))], axis=along))


def whole_of(array, axes, dim):
    for axis in reversed(axes):
        array = lax.all_gather(array, axis, axis=dim, tiled=True)
    return array


def sent_to_all(array, axis):
    copies = jnp.broadcast_to(array, (lax.axis_size(axis), *array.shape))
    return lax.all_to_all(copies, axis, split_axis=0, concat_axis=0, tiled=True)


def all_in_one(array, axis):
    leaves = jax.tree.leaves(array)
    turns = sorted(range(len(leaves)), key=lambda k: -leaves[k].size)
    width = (1, *leaves[turns[0]].shape)[-1]
    lines = [
        jnp.pad(leaves[k].reshape(-1), (0, -leaves[k].size % width)).reshape(-1, width)
        for k in turns
    ]
    both, at, found = (sent_to_all(jnp.concatenate(lines), axis), 0, {})
    for k, line in zip(turns, lines):
        section = both[:, at : at + len(line)].reshape(len(both), -1)
        found[k] = section[:, : leaves[k].size].reshape(-1, *leaves[k].shape)
        at += len(line)
    numbers = iter(range(len(leaves)))
    return jax.tree.map(lambda _: found[next(numbers)], array)


def joined_by_halves(pieces, combine):
    while len(jax.tree.leaves(pieces)[0]) > 1:
        pieces = jax.vmap(combine)(
            *(jax.tree.map(lambda part: part[side::2], pieces) for side in (0, 1))
        )
    return jax.tree.map(lambda part: part[0], pieces)


def entering(array, axis, combine, identity):
    length, here = (lax.axis_size(axis), lax.axis_index(axis))
    passed = jnp.arange(length) < here

    def kept(part, zero, own):
        part = jnp.where(
            passed.reshape(-1, *(1 for _ in own.shape)), part, jnp.asarray(zero, own.dtype)
        )
        return part

    pieces = all_in_one(array, axis)
    return joined_by_halves(jax.tree.map(kept, pieces, identity, array), combine)


def cut_along(array, dim, length):
    lengths = array.shape
    blocks = array.reshape(*lengths[:dim], length, lengths[dim] // length, *lengths[dim + 1 :])
    return jnp.moveaxis(blocks, dim, 0)


def sent_and_summed(array, axis, dim):
    length = lax.axis_size(axis)
    blocks = lax.all_to_all(cut_along(array, dim, length), axis, 0, 0, tiled=True)
    return jnp.sum(blocks.astype(jnp.float32), axis=0)


def joined_along(blocks, dim):
    lengths = list(blocks.shape[1:])
    lengths[dim] *= blocks.shape[0]
    return jnp.moveaxis(blocks, 0, dim).reshape(lengths)


def gathered_copies(array, axis, dim):
    blocks = sent_to_all(array, axis)
    return joined_along(blocks, dim)


def discrete(decay_real, decay_imag, log_step, in_real, in_imag):
    step_size = jnp.exp(log_step)[:, None]
    magnitude = jnp.exp(decay_real * step_size)
    angle = decay_imag * step_size
    power_re = magnitude * jnp.cos(angle)
    power_im = magnitude * jnp.sin(angle)
    denom = decay_real * decay_real + decay_imag * decay_imag
    ratio_re = ((power_re - 1.0) * decay_real + power_im * decay_imag) / denom
    ratio_im = (power_im * decay_real - (power_re - 1.0) * decay_imag) / denom
    drive_re = ratio_re[..., None] * in_real - ratio_im[..., None] * in_imag
    drive_im = ratio_re[..., None] * in_imag + ratio_im[..., None] * in_real
    return (power_re, power_im, drive_re, drive_im)


def combine(earlier, later):
    ar1, ai1, br1, bi1 = earlier
    ar2, ai2, br2, bi2 = later
    return (
        ar2 * ar1 - ai2 * ai1,
        ar2 * ai1 + ai2 * ar1,
        ar2 * br1 - ai2 * bi1 + br2,
        ar2 * bi1 + ai2 * br1 + bi2,
    )


def spread_blocks(matrix):
    groups = matrix.shape[0]
    unit_blocks = jnp.eye(groups, dtype=jnp.float32)[:, None, :, None]
    turned = jnp.transpose(matrix, (0, 2, 1))[:, :, None, :]
    return (unit_blocks * turned).reshape(groups * matrix.shape[2], groups * matrix.shape[1])


def local_states(power_re, power_im, drive_re, drive_im):
    rows, flat_size = drive_re.shape
    span = 8
    blocks = rows // span
    dr = drive_re.reshape(blocks, span, flat_size)
    di = drive_im.reshape(blocks, span, flat_size)
    cur_re = dr[:, 0]
    cur_im = di[:, 0]
    inner_re = [cur_re]
    inner_im = [cur_im]
    lift_re = [power_re]
    lift_im = [power_im]
    for index in range(1, span):
        cur_re, cur_im = (
            power_re * cur_re - power_im * cur_im + dr[:, index],
            power_re * cur_im + power_im * cur_re + di[:, index],
        )
        inner_re.append(cur_re)
        inner_im.append(cur_im)
        prev_re, prev_im = (lift_re[-1], lift_im[-1])
        lift_re.append(power_re * prev_re - power_im * prev_im)
        lift_im.append(power_re * prev_im + power_im * prev_re)
    inner_re = jnp.stack(inner_re, axis=1)
    inner_im = jnp.stack(inner_im, axis=1)
    lift_re = jnp.concatenate(lift_re, axis=0)[None]
    lift_im = jnp.concatenate(lift_im, axis=0)[None]
    block_re = jnp.broadcast_to(lift_re[0, span - 1][None], (blocks, flat_size))
    block_im = jnp.broadcast_to(lift_im[0, span - 1][None], (blocks, flat_size))
    totals = (block_re, block_im, cur_re, cur_im)
    distance = 1
    while distance < blocks:
        ones = jnp.ones((distance, flat_size), jnp.float32)
        zeros = jnp.zeros((distance, flat_size), jnp.float32)
        moved = (
            jnp.concatenate([ones, totals[0][:-distance]], axis=0),
            jnp.concatenate([zeros, totals[1][:-distance]], axis=0),
            jnp.concatenate([zeros, totals[2][:-distance]], axis=0),
            jnp.concatenate([zeros, totals[3][:-distance]], axis=0),
        )
        totals = combine(moved, totals)
        distance = distance * 2
    one_row = jnp.ones((1, flat_size), jnp.float32)
    zero_row = jnp.zeros((1, flat_size), jnp.float32)
    before_a_re = jnp.concatenate([one_row, totals[0][:-1]], axis=0)[:, None]
    before_a_im = jnp.concatenate([zero_row, totals[1][:-1]], axis=0)[:, None]
    before_re = jnp.concatenate([zero_row, totals[2][:-1]], axis=0)[:, None]
    before_im = jnp.concatenate([zero_row, totals[3][:-1]], axis=0)[:, None]
    state_real = inner_re + lift_re * before_re - lift_im * before_im
    state_imaginary = inner_im + lift_re * before_im + lift_im * before_re
    pw_re = lift_re * before_a_re - lift_im * before_a_im
    pw_im = lift_re * before_a_im + lift_im * before_a_re
    summary = (totals[0][-1], totals[1][-1], totals[2][-1], totals[3][-1])
    return (
        pw_re.reshape(rows, flat_size),
        pw_im.reshape(rows, flat_size),
        state_real.reshape(rows, flat_size),
        state_imaginary.reshape(rows, flat_size),
        summary,
    )


def on_device(
    mixer_in,
    residual,
    decay_real,
    decay_imag,
    log_step,
    in_real,
    in_imag,
    output_real,
    output_imaginary,
    skip,
    out_proj,
    norm_gain,
    w_gate,
    w_up,
    w_down,
):
    highest_precision = lax.Precision.HIGHEST
    whole_gate, whole_up = side_by_side((w_gate, w_up), SP, 0, 1)
    whole_down = whole_of(w_down, SP, 1)
    power_re, power_im, bar_re, bar_im = discrete(
        decay_real, decay_imag, log_step, in_real, in_imag
    )
    flat_size = decay_real.shape[0] * decay_real.shape[1]
    read_in = jnp.concatenate([spread_blocks(bar_re), spread_blocks(bar_im)], axis=1)
    signal = mixer_in.astype(jnp.float32)
    drive = jnp.dot(signal, read_in, precision=highest_precision)
    drive_re = drive[:, :flat_size]
    drive_im = drive[:, flat_size:]
    pw_re, pw_im, state_real, state_imaginary, summary = local_states(
        power_re.reshape(1, flat_size), power_im.reshape(1, flat_size), drive_re, drive_im
    )
    zero_line = jnp.zeros((flat_size,), jnp.float32)
    identity = (jnp.ones((flat_size,), jnp.float32), zero_line, zero_line, zero_line)
    _, _, hold_re, hold_im = entering(summary, SP, combine, identity)
    state_real = state_real + pw_re * hold_re[None] - pw_im * hold_im[None]
    state_imaginary = state_imaginary + pw_re * hold_im[None] + pw_im * hold_re[None]
    read_out = jnp.concatenate(
        [spread_blocks(output_real), -spread_blocks(output_imaginary)], axis=0
    )
    mixed_before_norm = jnp.dot(
        jnp.concatenate([state_real, state_imaginary], axis=1),
        read_out,
        precision=highest_precision,
    )
    mixed_before_norm = mixed_before_norm + skip[None] * signal
    activated = jax.nn.gelu(mixed_before_norm).astype(jnp.bfloat16)
    partial_value = jnp.dot(activated, out_proj, preferred_element_type=jnp.float32).astype(
        jnp.bfloat16
    )
    mixed = sent_and_summed(
        lax.optimization_barrier(partial_value).astype(jnp.float32).astype(jnp.bfloat16), "tp", 0
    ).astype(jnp.bfloat16)
    carried = residual.astype(jnp.float32) + mixed.astype(jnp.float32)
    scale = lax.rsqrt(jnp.mean(carried * carried, axis=-1, keepdims=True) + 1e-06)
    normed = (carried * scale * norm_gain).astype(jnp.bfloat16)
    full_rows = gathered_copies(normed, "tp", 0)
    gate = jnp.dot(full_rows, whole_gate, preferred_element_type=jnp.float32)
    up = jnp.dot(full_rows, whole_up, preferred_element_type=jnp.float32)
    hidden = (jax.nn.silu(gate) * up).astype(jnp.bfloat16)
    partial_value = jnp.dot(hidden, whole_down, preferred_element_type=jnp.float32).astype(
        jnp.bfloat16
    )
    down = sent_and_summed(
        lax.optimization_barrier(partial_value).astype(jnp.float32).astype(jnp.bfloat16), "tp", 0
    ).astype(jnp.bfloat16)
    return (carried + 0.5 * down.astype(jnp.float32)).astype(jnp.bfloat16)


def solution(mesh):
    finer = Mesh(mesh.devices.reshape(16, 4, mesh.shape["tp"]), ("sp_0", "sp_1", "tp"))
    return jax.shard_map(
        on_device,
        mesh=finer,
        in_specs=(
            P(SP, "tp"),
            P(SP_TP, None),
            P("tp", None),
            P("tp", None),
            P("tp"),
            P("tp", None, None),
            P("tp", None, None),
            P("tp", None, None),
            P("tp", None, None),
            P("tp"),
            P("tp", None),
            P(),
            P(SP, "tp"),
            P(SP, "tp"),
            P("tp", SP),
        ),
        out_specs=P(SP_TP, None),
        check_vma=False,
    )
```

profile of v0, /device:TPU:1, one launch (start us, length us, event | category | flops | bytes accessed | tf_op | source)
XLA Modules:
  0.0 289.7 jit_solution(17139990485783009736)
XLA Ops:
  6.5 1.6 pad_maximum_fusion
  8.2 0.7 exp.10
  8.8 0.8 cosine_multiply_fusion
  10.0 0.9 subtract_bitcast_fusion
  10.9 0.2 broadcast_multiply_fusion.2
  11.1 0.1 mul.1976
  11.2 0.1 mul.1981
  11.6 1.0 convolution_bitcast_fusion
  12.6 0.2 slice_bitcast_fusion.1
  12.8 0.6 fusion.80
  13.4 0.6 fusion.81
  14.0 0.3 multiply_subtract_fusion.3
  14.5 1.3 copy_add_fusion.1
  15.8 0.1 bitcast_add_fusion.2
  17.1 0.9 broadcast_in_dim.49
  18.0 19.3 %all-to-all-start = ((f32[64,4,512]{2,1,0:T(4,128)}), f32[64,4,512]{2,1,0:T(4,128)S(1)}, u32[]{:S(2)}, u32[]{:S(2)}) async-start(f32[64,4,512]{2,1,0:T(4,128)} %broadcast_in_dim.49), calls=%async_computation | async-start | bytes 1048576 | tf_op jit(solution)/shard_map/all_to_all | solution.py:26
  37.3 11.4 %all_gather.10 = bf16[704,128]{0,1:T(8,128)(2,1)} all-gather(bf16[704,32]{0,1:T(8,128)(2,1)S(1)} %copy-done.14), channel_id=1, replica_groups=mesh['sp_0'=16,'sp_1'=4,'tp'=8] {'sp_1'}, dimensions={1}, use_global_device_ids=true | all-gather | bytes 225280 | tf_op jit(solution)/shard_map/all_gather | solution.py:20
  48.7 0.8 copy.114
  49.5 0.8 copy.103
  50.3 0.8 copy.109
  51.2 0.1 copy.111
  51.4 0.1 copy.112
  51.5 0.1 copy.113
  51.7 0.7 concatenate.135
  52.4 0.7 concatenate.130
  53.1 0.8 copy.100
  53.8 0.8 copy.101
  54.6 0.8 copy.102
  55.4 0.8 copy.98
  56.2 0.8 copy.99
  57.0 0.9 copy.115
  57.9 0.8 broadcast_multiply_fusion
  58.7 0.9 mul.2189
  59.6 0.9 neg.11
  60.5 0.7 concatenate.134
  61.2 1.6 stack.5
  62.8 2.9 %stack.4 = f32[64,8,512]{2,1,0:T(8,128)S(1)} concatenate(f32[64,1,512]{2,1,0:T(1,128)S(1)} %get-tuple-element.60, f32[64,1,512]{2,1,0:T(1,128)} %copy.98, f32[64,1,512]{2,1,0:T(1,128)} %copy.99, f32[64,1,512]{2,1,0:T(1,128)} %copy.100, f32[64,1,512]{2,1,0:T(1,128)} %copy.101, f32[64,1,512]{2,1,0:T(1,128)} %copy.102, f32[64,1,512]{2,1,0:T(1,128)} %copy.103, ...), dimensions={1} | concatenate | bytes 2097152 | tf_op jit(solution)/shard_map/stack | solution.py:145
  65.7 0.5 iota_compare_fusion.1
  66.3 5.0 %all-to-all-done = f32[64,4,512]{2,1,0:T(4,128)S(1)} async-done(((f32[64,4,512]{2,1,0:T(4,128)}), f32[64,4,512]{2,1,0:T(4,128)S(1)}, u32[]{:S(2)}, u32[]{:S(2)}) %all-to-all-start) | async-done | bytes 524320 | tf_op jit(solution)/shard_map/all_to_all | solution.py:26
  71.2 0.4 fusion.82
  71.6 1.4 fusion.67
  73.1 1.5 slice.365
  74.6 1.5 slice.366
  76.2 0.6 slice.368
  76.8 0.6 slice.369
  77.5 0.6 slice.390
  78.2 0.6 slice.393
  78.8 1.0 multiply_subtract_fusion.4
  80.7 1.5 fusion.18
  82.3 1.8 fusion.40
  84.2 0.7 convolution_convert_fusion
  84.9 33.5 %all_to_all.20 = bf16[8,64,2048]{2,1,0:T(8,128)(2,1)S(1)} all-to-all(bf16[8,64,2048]{2,1,0:T(8,128)(2,1)S(1)} %bitcast.189), channel_id=1, replica_groups=mesh['sp_0'=16,'sp_1'=4,'tp'=8] {'tp'}, dimensions={0} | all-to-all | bytes 4194304 | tf_op jit(solution)/shard_map/all_to_all | solution.py:76
  118.3 0.4 reduce_sum.33
  118.7 0.6 copy-done.1
  119.3 0.2 multiply_reduce_fusion
  119.6 0.2 broadcast_in_dim.94
  119.9 29.6 %all_to_all.21 = bf16[8,64,2048]{2,1,0:T(8,128)(2,1)S(1)} all-to-all(bf16[8,64,2048]{2,1,0:T(8,128)(2,1)S(1)} %broadcast_in_dim.94), channel_id=1, replica_groups=mesh['sp_0'=16,'sp_1'=4,'tp'=8] {'tp'}, dimensions={0} | all-to-all | bytes 4194304 | tf_op jit(solution)/shard_map/all_to_all | solution.py:26
  149.5 11.3 %all-gather.3.cloned.1.call-done = bf16[2048,1408]{1,0:T(8,128)(2,1)} async-done(((bf16[32,1408]{1,0:T(8,128)(2,1)}), bf16[2048,1408]{1,0:T(8,128)(2,1)}) %all-gather.3.cloned.1.call-update) | async-done | bytes 5767184 | tf_op jit(solution)/shard_map/all_gather | solution.py:14
  160.8 4.7 %fusion.2 = f32[512,704]{0,1:T(8,128)} fusion(bf16[512,2048]{1,0:T(8,128)(2,1)S(1)} %bitcast.194, bf16[2048,1408]{1,0:T(8,128)(2,1)} %all-gather.3.cloned.1.call-done), kind=kOutput, calls=%fused_computation.2 | convolution fusion | flops 1476395008 | bytes 6684672 | tf_op jit(solution)/shard_map/dot_general | solution.py:241
  165.5 66.9 %all-gather.5.cloned.1.call-done = bf16[704,2048]{0,1:T(8,128)(2,1)} async-done(((bf16[704,128]{0,1:T(8,128)(2,1)}), bf16[704,2048]{0,1:T(8,128)(2,1)}) %all-gather.5.cloned.1.call-update) | async-done | bytes 2883600 | tf_op jit(solution)/shard_map/all_gather | solution.py:20
  232.4 9.3 %convolution_convert_fusion.1 = bf16[512,2048]{1,0:T(8,128)(2,1)} fusion(bf16[704,2048]{0,1:T(8,128)(2,1)} %all-gather.5.cloned.1.call-done, bf16[512,2048]{1,0:T(8,128)(2,1)S(1)} %bitcast.195, bf16[2048,1408]{1,0:T(8,128)(2,1)} %all-gather.3.cloned.1.call-done, f32[512,704]{0,1:T(8,128)} %fusion.2), kind=kOutput, calls=%fused_computation.5 | convolution fusion | flops 2956001280 | bytes 11927552 | tf_op jit(solution)/shard_map/dot_general | solution.py:244
  241.7 40.0 %all_to_all.22 = bf16[8,64,2048]{2,1,0:T(8,128)(2,1)S(1)} all-to-all(bf16[8,64,2048]{2,1,0:T(8,128)(2,1)} %bitcast.196), channel_id=1, replica_groups=mesh['sp_0'=16,'sp_1'=4,'tp'=8] {'tp'}, dimensions={0} | all-to-all | bytes 4194304 | tf_op jit(solution)/shard_map/all_to_all | solution.py:76
  281.7 0.4 reduce_sum.35
  282.1 0.8 add_convert_fusion
  (128 shorter events, 2.9 us)
Async XLA Ops:
  6.5 77.6 %copy-start = (bf16[128,2048]{1,0:T(8,128)(2,1)S(1)}, bf16[128,2048]{1,0:T(8,128)(2,1)}, u32[]{:S(2)}) copy-start(bf16[128,2048]{1,0:T(8,128)(2,1)} %param.25) | copy-start | bytes 1572868
  6.5 5.0 %copy-start.10 = (bf16[512,128]{1,0:T(8,128)(2,1)S(1)}, bf16[512,128]{1,0:T(8,128)(2,1)}, u32[]{:S(2)}) copy-start(bf16[512,128]{1,0:T(8,128)(2,1)} %param.15) | copy-start | bytes 393220
  6.5 154.3 %all-gather.3.cloned.1.call-start = ((), (), s32[]{:S(2)}) async-start(), calls=%async_computation.4 | async-start | bytes 5857280 | tf_op jit(solution)/shard_map/all_gather | solution.py:14
  10.0 2.6 copy-start.15
  11.5 1.3 copy-start.12
  16.8 20.5 %copy-start.14 = (bf16[704,32]{0,1:T(8,128)(2,1)S(1)}, bf16[704,32]{0,1:T(8,128)(2,1)}, u32[]{:S(2)}) copy-start(bf16[704,32]{0,1:T(8,128)(2,1)} %param.29) | copy-start | bytes 135172
  18.0 53.3 %all-to-all-start = ((f32[64,4,512]{2,1,0:T(4,128)}), f32[64,4,512]{2,1,0:T(4,128)S(1)}, u32[]{:S(2)}, u32[]{:S(2)}) async-start(f32[64,4,512]{2,1,0:T(4,128)} %broadcast_in_dim.49), calls=%async_computation | async-start | bytes 1048576 | tf_op jit(solution)/shard_map/all_to_all | solution.py:26
  37.2 195.2 %all-gather.5.cloned.1.call-start = ((), (), s32[]{:S(2)}) async-start(), calls=%async_computation.5 | async-start | bytes 3342336 | tf_op jit(solution)/shard_map/all_gather | solution.py:20
  49.5 8.3 %copy-start.13 = (f32[8,16,64]{2,1,0:T(8,128)S(1)}, f32[8,16,64]{2,1,0:T(8,128)}, u32[]{:S(2)}) copy-start(f32[8,16,64]{2,1,0:T(8,128)} %param.23) | copy-start | bytes 98308
  54.6 6.5 %copy-start.5 = (f32[64,1,512]{2,1,0:T(1,128)S(1)}, f32[64,1,512]{2,1,0:T(1,128)}, u32[]{:S(2)}) copy-start(f32[64,1,512]{2,1,0:T(1,128)} %copy.114) | copy-start | bytes 393220
  54.6 6.5 %copy-start.6 = (f32[64,1,512]{2,1,0:T(1,128)S(1)}, f32[64,1,512]{2,1,0:T(1,128)}, u32[]{:S(2)}) copy-start(f32[64,1,512]{2,1,0:T(1,128)} %copy.109) | copy-start | bytes 393220
  54.6 6.5 %copy-start.7 = (f32[64,1,512]{2,1,0:T(1,128)S(1)}, f32[64,1,512]{2,1,0:T(1,128)}, u32[]{:S(2)}) copy-start(f32[64,1,512]{2,1,0:T(1,128)} %get-tuple-element.127) | copy-start | bytes 393220
  71.6 9.0 %copy-start.2 = (f32[64,512]{1,0:T(8,128)S(1)}, f32[64,512]{1,0:T(8,128)}, u32[]{:S(2)}) copy-start(f32[64,512]{1,0:T(8,128)} %concatenate.135) | copy-start | bytes 393220
  71.6 9.0 %copy-start.3 = (f32[64,512]{1,0:T(8,128)S(1)}, f32[64,512]{1,0:T(8,128)}, u32[]{:S(2)}) copy-start(f32[64,512]{1,0:T(8,128)} %concatenate.130) | copy-start | bytes 393220
  71.6 9.0 %copy-start.4 = (f32[64,512]{1,0:T(8,128)S(1)}, f32[64,512]{1,0:T(8,128)}, u32[]{:S(2)}) copy-start(f32[64,512]{1,0:T(8,128)} %concatenate.134) | copy-start | bytes 393220
  80.7 1.6 copy-start.8
  80.7 1.6 copy-start.9
  80.7 1.6 copy-start.11
  80.7 1.6 copy-start.17
  118.3 1.0 copy-start.1
  118.3 1.1 copy-start.16
Sparse Core Ops, SparseCore 0:
  10.3 150.4 all-gather.2
  162.9 69.5 all-gather.4
where the time goes:
time: 291 us; the launch traced here: 290 us
  blocking collectives  114 us (39%)
  waiting for transfers between devices  83.3 us (29%)
  local copies, waits for them, and re-layouts  27.4 us (9%)
  starting transfers between devices  19.3 us (7%)
  matrix products  17.5 us (6%)
  between operations  14.1 us (5%)
  other arithmetic  13.5 us (5%)
    all_to_all x2, blocking collectives, sent_and_summed(): lax.all_to_all(cut_along(array, dim, length), axis, 0, 0, tiled=True)  73.5 us
    all_gather x1, waiting for transfers between devices, whole_of(): array = lax.all_gather(array, axis, axis=dim, tiled=True)  66.9 us
    all_to_all x1, blocking collectives, sent_to_all(): return lax.all_to_all(copies, axis, split_axis=0, concat_axis=0, tiled=True)  29.6 us
    all_to_all x1, starting transfers between devices, sent_to_all(): return lax.all_to_all(copies, axis, split_axis=0, concat_axis=0, tiled=True)  19.3 us
    all_gather x1, blocking collectives, whole_of(): array = lax.all_gather(array, axis, axis=dim, tiled=True)  11.4 us
    all_gather x1, waiting for transfers between devices, side_by_side(): result = lax.all_gather(both, axis, axis=dim, tiled=True)  11.3 us
    dot_general x1, matrix products, on_device(): jnp.dot(hidden, whole_down, preferred_element_type=jnp.float32)  9.27 us
    slice x40, local copies, waits for them, and re-layouts, joined_by_halves(): part[side::2]  6.34 us
  transfers between devices with their start and end apart: 3, of which 3 were waited for; matrix products, arithmetic and copies ran while one was open for 16% of the time, Pallas kernels for 0%

commit v1 on v0

v1 whole, which is shorter than its diff:
```python
import functools

import jax
import jax.numpy as jnp
from jax import lax
from jax.experimental import pallas as pl
from jax.experimental.pallas import tpu as pltpu
from jax.sharding import Mesh
from jax.sharding import PartitionSpec as P

SP = ("sp_0", "sp_1")
SP_TP = ("sp_0", "sp_1", "tp")
MESH = pl.DeviceIdType.MESH
F32 = jnp.float32
BF16 = jnp.bfloat16

NZ = 16
NY = 4
NX = 4
NT = 8
HALF = NZ // 2
D = 2048
TOK = 512
ROWS = TOK // NT
FL = 512
CHD = 128
FFD = 704
KB = 32
GU = 2 * FFD
Q = 176


def discrete(decay_real, decay_imag, log_step):
    step_size = jnp.exp(log_step)[:, None]
    magnitude = jnp.exp(decay_real * step_size)
    angle = decay_imag * step_size
    power_re = magnitude * jnp.cos(angle)
    power_im = magnitude * jnp.sin(angle)
    denom = decay_real * decay_real + decay_imag * decay_imag
    ratio_re = ((power_re - 1.0) * decay_real + power_im * decay_imag) / denom
    ratio_im = (power_im * decay_real - (power_re - 1.0) * decay_imag) / denom
    return jnp.stack([power_re, power_im, ratio_re, ratio_im])


def cmul(a, b):
    return (a[0] * b[0] - a[1] * b[1], a[0] * b[1] + a[1] * b[0])


def cadd(a, b):
    return (a[0] + b[0], a[1] + b[1])


def pieces(v):
    hi = v.astype(BF16)
    lo = (v - hi.astype(F32)).astype(BF16)
    return hi, lo


def dot(a, b):
    return jnp.dot(a, b, preferred_element_type=F32)


def dot_t(a, b):
    return lax.dot_general(a, b, (((1,), (1,)), ((), ())), preferred_element_type=F32)


def packed(row):
    return jnp.concatenate([row[:, i * 128 : (i + 1) * 128] for i in range(4)], axis=0)


def flat(block):
    return jnp.concatenate([block[i : i + 1] for i in range(4)], axis=1)


def kernel(
    x_ref, cf_ref, inr_ref, ini_ref, our_ref, oui_ref, skip_ref, op_ref, gain_ref,
    res_ref, wg_ref, wu_ref, wd_ref, out_ref,
    wgu, wdn, dy, opall, sb, tb, act, acts, nf, hid, part, pr, ps, rs1, rs2, rs3,
    ur, ui, mr, mi, er, ei, pcr, pci, carried,
    g_recv, gz_send, gy_send, d_recv, dz_send, dy_recv, dy_send,
    o_recv, o_send, s_recv, s_send, t_recv, t_send, a_recv, a_send,
    n_recv, n_send, p_recv, p_send, r_recv, r_send,
):
    z = lax.axis_index("sp_0")
    y = lax.axis_index("sp_1")
    t = lax.axis_index("tp")
    x = t // 2
    c = t % 2
    yp = (y + 1 + 2 * c) % NY
    ym = (y + 3 + 2 * c) % NY
    y2 = (y + 2) % NY
    zp = (z + 1 + (NZ - 2) * c) % NZ
    zm = (z + NZ - 1 + 2 * c) % NZ
    xp = (x + 1 + 2 * c) % NX
    xm = (x + 3 + 2 * c) % NX
    x2 = (x + 2) % NX
    other = 1 - c
    tpp = xp * 2 + c
    tpm = xm * 2 + c
    tp2 = x2 * 2 + c
    tpo = x * 2 + other
    sent = []

    def copy(src, dst, ss, rs, **dev):
        return pltpu.make_async_remote_copy(
            src_ref=src, dst_ref=dst, send_sem=ss, recv_sem=rs, device_id=dev, device_id_type=MESH
        )

    def send(src, dst, ss, rs, **dev):
        cp = copy(src, dst, ss, rs, **dev)
        cp.start()
        sent.append(cp)

    def arrived(dst, ss, rs, **dev):
        copy(dst, dst, ss, rs, **dev).wait_recv()

    barrier = pltpu.get_barrier_semaphore()
    for k in range(1, NT):
        pl.semaphore_signal(barrier, inc=1, device_id={"tp": (t + k) % NT}, device_id_type=MESH)
    for k in range(1, NY):
        pl.semaphore_signal(barrier, inc=1, device_id={"sp_1": (y + k) % NY}, device_id_type=MESH)
    for k in range(1, NZ):
        pl.semaphore_signal(barrier, inc=1, device_id={"sp_0": (z + k) % NZ}, device_id_type=MESH)

    own = z * NY + y
    wgu[own, :, 0:640] = wg_ref[:, 0:640]
    wgu[own, :, 640:1280] = wu_ref[:, 0:640]
    wgu[own, :, 1280:1408] = jnp.concatenate([wg_ref[:, 640:704], wu_ref[:, 640:704]], axis=1)
    dy[y] = jnp.concatenate([wd_ref[q * Q : (q + 1) * Q] for q in range(4)], axis=1)
    opall[t] = op_ref[...]

    pl.semaphore_wait(barrier, NT - 1 + NY - 1 + NZ - 1)

    def g_blk(zb, yb):
        return wgu.at[zb * NY + yb]

    def g_z_forward(zb, chain, s):
        blk = g_blk(zb, y)
        send(blk, blk, gz_send.at[chain * HALF + s], g_recv.at[zb * NY + y],
             sp_0=zp if chain == 0 else zm)

    def g_y_start(zb, o):
        blk = g_blk(zb, y)
        send(blk, blk, gy_send.at[3 * o], g_recv.at[zb * NY + y], sp_1=yp)
        send(blk, blk, gy_send.at[3 * o + 1], g_recv.at[zb * NY + y], sp_1=ym)

    def g_y_forward(zb, o):
        blk = g_blk(zb, ym)
        arrived(blk, gy_send.at[3 * o + 2], g_recv.at[zb * NY + ym], sp_1=ym)
        send(blk, blk, gy_send.at[3 * o + 2], g_recv.at[zb * NY + ym], sp_1=yp)

    def g_y_finish(zb, o):
        for yb in (yp, y2):
            arrived(g_blk(zb, yb), gy_send.at[3 * o], g_recv.at[zb * NY + yb], sp_1=yp)

    def chain_block(chain, s):
        toward = zm - z if chain == 0 else zp - z
        return (z + NZ * NZ + s * toward) % NZ

    def d_z_forward(zb, chain, s):
        send(wdn.at[zb], wdn.at[zb], dz_send.at[chain * HALF + s], d_recv.at[zb],
             sp_0=zp if chain == 0 else zm)

    def d_start():
        for k in range(1, NY):
            yk = (y + k) % NY
            arrived(dy.at[yk], dy_send.at[k], dy_recv.at[yk], sp_1=yk)
        for q in range(4):
            wdn[z, q * Q : (q + 1) * Q, :] = jnp.concatenate(
                [dy[b, :, q * KB : (q + 1) * KB] for b in range(NY)], axis=1
            )
        d_z_forward(z, 0, 0)
        d_z_forward(z, 1, 0)

    def steps(s):
        return [(0, s)] + ([(1, s)] if s < HALF else [])

    def order(chain, s):
        return 0 if s == 0 else 2 * s - 1 + chain

    def tick(s):
        for chain, s_ in steps(s):
            zb = chain_block(chain, s_)
            arrived(g_blk(zb, y), gz_send.at[0], g_recv.at[zb * NY + y], sp_0=zm)
            if s_ < (HALF if chain == 0 else HALF - 1):
                g_z_forward(zb, chain, s_)
            g_y_start(zb, order(chain, s_))
        if s == 1:
            g_y_forward(z, 0)
        else:
            for chain, s_ in steps(s - 1):
                g_y_forward(chain_block(chain, s_), order(chain, s_))
        for chain, s_ in steps(s):
            zb = chain_block(chain, s_)
            arrived(wdn.at[zb], dz_send.at[0], d_recv.at[zb], sp_0=zm)
            if s_ < (HALF if chain == 0 else HALF - 1):
                d_z_forward(zb, chain, s_)

    def tp_start(buf, recv, ssem):
        send(buf.at[t], buf.at[t], ssem.at[0], recv.at[t], tp=tpp)
        send(buf.at[t], buf.at[t], ssem.at[1], recv.at[t], tp=tpm)
        send(buf.at[t], buf.at[t], ssem.at[2], recv.at[t], tp=tpo)

    def tp_forward(buf, recv, ssem):
        arrived(buf.at[tpm], ssem.at[0], recv.at[tpm], tp=tpm)
        send(buf.at[tpm], buf.at[tpm], ssem.at[3], recv.at[tpm], tp=tpp)
        send(buf.at[tpm], buf.at[tpm], ssem.at[4], recv.at[tpm], tp=tpo)
        arrived(buf.at[tpp], ssem.at[0], recv.at[tpp], tp=tpp)
        send(buf.at[tpp], buf.at[tpp], ssem.at[5], recv.at[tpp], tp=tpo)

    def tp_last(buf, recv, ssem):
        arrived(buf.at[tp2], ssem.at[0], recv.at[tp2], tp=tpm)
        send(buf.at[tp2], buf.at[tp2], ssem.at[6], recv.at[tp2], tp=tpo)

    def tp_finish(buf, recv, ssem):
        for xb in (x, xp, xm, x2):
            b = xb * 2 + other
            arrived(buf.at[b], ssem.at[0], recv.at[b], tp=tpo)

    for k in range(1, NY):
        yk = (y + k) % NY
        send(dy.at[y], dy.at[y], dy_send.at[k], dy_recv.at[y], sp_1=yk)
    g_z_forward(z, 0, 0)
    g_z_forward(z, 1, 0)
    g_y_start(z, 0)
    tp_start(opall, o_recv, o_send)

    a = (cf_ref[0:1], cf_ref[1:2])
    ratio = (cf_ref[2:3], cf_ref[3:4])
    powers = [a]
    for _ in range(7):
        powers.append(cmul(powers[-1], a))
    lift = tuple(jnp.concatenate([p[i] for p in powers], axis=0) for i in (0, 1))
    row8 = lax.broadcasted_iota(jnp.int32, (8, FL), 0)
    masked = []
    for k in (1, 2, 4):
        p = powers[k - 1]
        masked.append(tuple(jnp.where(row8 >= k, jnp.broadcast_to(v, (8, FL)), 0.0) for v in p))

    spread = (
        lax.broadcasted_iota(jnp.int32, (16, CHD), 1) % 16
        == lax.broadcasted_iota(jnp.int32, (16, CHD), 0)
    ).astype(F32).astype(BF16)
    block = (
        lax.broadcasted_iota(jnp.int32, (FL, CHD), 0) // 64
        == lax.broadcasted_iota(jnp.int32, (FL, CHD), 1) // 16
    )
    signal = x_ref[...]
    for src, dst in ((inr_ref, ur), (ini_ref, ui)):
        total = None
        for piece in pieces(src[...]):
            wide = jnp.where(block, dot(piece, spread), 0.0).astype(BF16)
            term = dot_t(signal, wide)
            total = term if total is None else total + term
        dst[...] = total

    def tile_step(i, carry):
        for j in range(4):
            rows = pl.ds(pl.multiple_of(i * 32 + j * 8, 8), 8)
            v = cmul(ratio, (ur[rows, :], ui[rows, :]))
            for k, m in zip((1, 2, 4), masked):
                v = cadd(v, cmul(m, (pltpu.roll(v[0], k, 0), pltpu.roll(v[1], k, 0))))
            ur[rows, :] = v[0]
            ui[rows, :] = v[1]
            er[pl.ds(i * 4 + j, 1), :] = v[0][7:8]
            ei[pl.ds(i * 4 + j, 1), :] = v[1][7:8]
        return carry

    lax.fori_loop(0, TOK // 32, tile_step, 0)

    row64 = lax.broadcasted_iota(jnp.int32, (64, FL), 0)
    e = (er[...], ei[...])
    ladder = []
    p = powers[7]
    for k in (1, 2, 4, 8, 16, 32):
        ladder.append(p)
        moved = tuple(jnp.where(row64 >= k, pltpu.roll(v, k, 0), 0.0) for v in e)
        e = cadd(e, cmul(p, moved))
        p = cmul(p, p)
    er[...] = e[0]
    ei[...] = e[1]
    a512 = (packed(p[0]), packed(p[1]))
    last = (e[0][63:64], e[1][63:64])
    sb[y, 0:4, :] = packed(last[0])
    sb[y, 4:8, :] = packed(last[1])
    for k in range(1, NY):
        send(sb.at[y], sb.at[y], s_send.at[k], s_recv.at[y], sp_1=(y + k) % NY)

    d_start()

    lead = (jnp.ones((64, FL), F32), jnp.zeros((64, FL), F32))
    for b, q in enumerate(ladder):
        more = cmul(q, lead)
        bit = (row64 // (1 << b)) % 2 == 1
        lead = tuple(jnp.where(bit, m, v) for m, v in zip(more, lead))
    pcr[...] = lead[0]
    pci[...] = lead[1]

    for k in range(1, NY):
        yk = (y + k) % NY
        arrived(sb.at[yk], s_send.at[k], s_recv.at[yk], sp_1=yk)
    whole = (jnp.zeros((4, 128), F32), jnp.zeros((4, 128), F32))
    before = whole
    ahead = (jnp.ones((4, 128), F32), jnp.zeros((4, 128), F32))
    for b in range(NY):
        own_b = (sb[b, 0:4, :], sb[b, 4:8, :])
        whole = cadd(cmul(a512, whole), own_b)
        inside = b < y
        step_b = cadd(cmul(a512, before), own_b)
        before = tuple(jnp.where(inside, n, v) for n, v in zip(step_b, before))
        step_a = cmul(a512, ahead)
        ahead = tuple(jnp.where(inside, n, v) for n, v in zip(step_a, ahead))
    a2 = cmul(a512, a512)
    a4 = cmul(a2, a2)
    tb[z, 0:4, :] = whole[0]
    tb[z, 4:8, :] = whole[1]
    for k in range(1, NZ):
        send(tb.at[z], tb.at[z], t_send.at[k], t_recv.at[z], sp_0=(z + k) % NZ)

    spread2 = (
        lax.broadcasted_iota(jnp.int32, (64, FL), 1) % 64
        == lax.broadcasted_iota(jnp.int32, (64, FL), 0)
    ).astype(F32).astype(BF16)
    block2 = (
        lax.broadcasted_iota(jnp.int32, (CHD, FL), 0) // 16
        == lax.broadcasted_iota(jnp.int32, (CHD, FL), 1) // 64
    )
    for k, (src, sign) in enumerate(((our_ref, 1.0), (oui_ref, -1.0))):
        hi, lo = pieces(src[...] * sign)
        mr[k] = jnp.where(block2, dot(hi, spread2), 0.0).astype(BF16)
        mi[k] = jnp.where(block2, dot(lo, spread2), 0.0).astype(BF16)

    tick(1)

    for k in range(1, NZ):
        zk = (z + k) % NZ
        arrived(tb.at[zk], t_send.at[k], t_recv.at[zk], sp_0=zk)
    hold = (jnp.zeros((4, 128), F32), jnp.zeros((4, 128), F32))
    for b in range(NZ - 1):
        step_h = cadd(cmul(a4, hold), (tb[b, 0:4, :], tb[b, 4:8, :]))
        hold = tuple(jnp.where(b < z, n, v) for n, v in zip(step_h, hold))
    hold = cadd(cmul(ahead, hold), before)
    hold = (flat(hold[0]), flat(hold[1]))
    enter = cmul((pcr[...], pci[...]), hold)
    prev = tuple(jnp.where(row64 >= 1, pltpu.roll(v[...], 1, 0), 0.0) for v in (er, ei))
    enter = cadd(enter, prev)
    pcr[...] = enter[0]
    pci[...] = enter[1]

    def read_step(i, carry):
        re, im = [], []
        for j in range(16):
            k = i * 16 + j
            rows = pl.ds(pl.multiple_of(k * 8, 8), 8)
            w = (pcr[pl.ds(k, 1), :], pci[pl.ds(k, 1), :])
            v = cadd((ur[rows, :], ui[rows, :]), cmul(lift, w))
            re.append(v[0])
            im.append(v[1])
        total = None
        for k, v in enumerate((re, im)):
            hi, lo = pieces(jnp.concatenate(v, axis=0))
            term = dot_t(hi, mr[k]) + dot_t(hi, mi[k]) + dot_t(lo, mr[k])
            total = term if total is None else total + term
        rows = pl.ds(pl.multiple_of(i * 128, 128), 128)
        pre = total + skip_ref[...] * x_ref[rows, :].astype(F32)
        inner = 0.7978845608028654 * (pre + 0.044715 * (pre * pre * pre))
        val = (pre * (0.5 * (1.0 + jnp.tanh(inner)))).astype(BF16)
        act[2 * i] = val[0:64]
        act[2 * i + 1] = val[64:128]
        return carry

    lax.fori_loop(0, 4, read_step, 0)
    for k in range(1, NT):
        tk = (t + k) % NT
        send(act.at[tk], acts.at[t], a_send.at[k], a_recv.at[t], tp=tk)
    acts[t] = act[t]

    tp_forward(opall, o_recv, o_send)
    tick(2)
    tp_last(opall, o_recv, o_send)
    tp_finish(opall, o_recv, o_send)

    for k in range(1, NT):
        tk = (t + k) % NT
        arrived(acts.at[tk], a_send.at[k], a_recv.at[tk], tp=tk)

    def mix_step(j, squares):
        cols = pl.ds(pl.multiple_of(j * 256, 256), 256)
        total = jnp.zeros((ROWS, 256), F32)
        for b in range(NT):
            total = total + dot(acts[b], opall[b, :, cols]).astype(BF16).astype(F32)
        v = res_ref[:, cols].astype(F32) + total.astype(BF16).astype(F32)
        carried[:, cols] = v
        return squares + jnp.sum(v * v, axis=1, keepdims=True)

    squares = lax.fori_loop(0, D // 256, mix_step, jnp.zeros((ROWS, 1), F32))
    scale = lax.rsqrt(squares * (1.0 / D) + 1e-06)
    nf[t] = (carried[...] * scale * gain_ref[...]).astype(BF16)
    tp_start(nf, n_recv, n_send)
    tick(3)
    tp_forward(nf, n_recv, n_send)
    tick(4)
    tp_last(nf, n_recv, n_send)
    tp_finish(nf, n_recv, n_send)
    for s in range(5, HALF + 1):
        tick(s)
    for chain, s_ in steps(HALF):
        g_y_forward(chain_block(chain, s_), order(chain, s_))
    g_y_finish(z, 0)
    for s in range(1, HALF + 1):
        for chain, s_ in steps(s):
            g_y_finish(chain_block(chain, s_), order(chain, s_))

    def up_step(j, carry):
        c0 = pl.ds(pl.multiple_of(j * 128, 128), 128)
        c1 = pl.ds(pl.multiple_of(640 + j * 128, 128), 128)
        w = jnp.concatenate(
            [wgu[:, :, c0].reshape(D, 128), wgu[:, :, c1].reshape(D, 128)], axis=1
        )
        v = dot(nf[...].reshape(TOK, D), w)
        g = v[:, 0:128]
        hid[:, c0] = (g / (1.0 + jnp.exp(-g)) * v[:, 128:256]).astype(BF16)
        return carry

    lax.fori_loop(0, 5, up_step, 0)
    v = dot(nf[...].reshape(TOK, D), wgu[:, :, 1280:1408].reshape(D, 128))
    tail = v / (1.0 + jnp.exp(-v)) * pltpu.roll(v, 64, 1)
    hid[:, 640:704] = tail[:, 0:64].astype(BF16)

    def down_step(j, carry):
        w = jnp.concatenate([wdn[2 * j], wdn[2 * j + 1]], axis=1)
        cols = pl.ds(pl.multiple_of(j * 256, 256), 256)
        part[:, :, cols] = dot(hid[...], w).astype(BF16).reshape(NT, ROWS, 256)
        return carry

    lax.fori_loop(0, NZ // 2, down_step, 0)

    targets = (x2, xm, xp, x)
    for k, xb in enumerate(targets):
        send(part.at[xb * 2 + other], pr.at[xb], p_send.at[k], p_recv.at[xb], tp=tpo)

    def pair(xb):
        arrived(pr.at[xb], p_send.at[0], p_recv.at[xb], tp=tpo)
        return part[xb * 2 + c].astype(F32) + pr[xb].astype(F32)

    ps[0] = pair(x2).astype(BF16)
    send(ps.at[0], rs1, r_send.at[0], r_recv.at[0], tp=tpp)
    ps[1] = pair(xm).astype(BF16)
    send(ps.at[1], rs2, r_send.at[1], r_recv.at[1], tp=tpm)
    near = pair(xp)
    arrived(rs1, r_send.at[0], r_recv.at[0], tp=tpm)
    ps[2] = (near + rs1[...].astype(F32)).astype(BF16)
    send(ps.at[2], rs3, r_send.at[2], r_recv.at[2], tp=tpp)
    mine = pair(x)
    arrived(rs2, r_send.at[1], r_recv.at[1], tp=tpp)
    arrived(rs3, r_send.at[2], r_recv.at[2], tp=tpm)
    down = (mine + rs2[...].astype(F32) + rs3[...].astype(F32)).astype(BF16)
    out_ref[...] = (carried[...] + 0.5 * down.astype(F32)).astype(BF16)

    for cp in sent:
        cp.wait_send()


def on_device(
    mixer_in, residual, decay_real, decay_imag, log_step, in_real, in_imag,
    output_real, output_imaginary, skip, out_proj, norm_gain, w_gate, w_up, w_down,
):
    cf = discrete(decay_real, decay_imag, log_step).reshape(4, FL)
    vmem = pltpu.VMEM
    dma = pltpu.SemaphoreType.DMA
    scratch = [
        vmem((NZ * NY, KB, GU), BF16),
        vmem((NZ, FFD, 128), BF16),
        vmem((NY, Q, 128), BF16),
        vmem((NT, CHD, D), BF16),
        vmem((NY, 8, 128), F32),
        vmem((NZ, 8, 128), F32),
        vmem((NT, ROWS, CHD), BF16),
        vmem((NT, ROWS, CHD), BF16),
        vmem((NT, ROWS, D), BF16),
        vmem((TOK, FFD), BF16),
        vmem((NT, ROWS, D), BF16),
        vmem((NX, ROWS, D), BF16),
        vmem((3, ROWS, D), BF16),
        vmem((ROWS, D), BF16),
        vmem((ROWS, D), BF16),
        vmem((ROWS, D), BF16),
        vmem((TOK, FL), F32),
        vmem((TOK, FL), F32),
        vmem((2, CHD, FL), BF16),
        vmem((2, CHD, FL), BF16),
        vmem((64, FL), F32),
        vmem((64, FL), F32),
        vmem((64, FL), F32),
        vmem((64, FL), F32),
        vmem((ROWS, D), F32),
        dma((NZ * NY,)), dma((NZ,)), dma((3 * NZ,)), dma((NZ,)), dma((NZ,)),
        dma((NY,)), dma((NY,)),
        dma((NT,)), dma((7,)), dma((NY,)), dma((NY,)), dma((NZ,)), dma((NZ,)),
        dma((NT,)), dma((NT,)), dma((NT,)), dma((7,)), dma((NX,)), dma((NX,)),
        dma((3,)), dma((3,)),
    ]
    return pl.pallas_call(
        kernel,
        out_shape=jax.ShapeDtypeStruct((ROWS, D), BF16),
        in_specs=[pl.BlockSpec(memory_space=vmem)] * 13,
        out_specs=pl.BlockSpec(memory_space=vmem),
        scratch_shapes=scratch,
        compiler_params=pltpu.CompilerParams(
            collective_id=0, has_side_effects=True, vmem_limit_bytes=60 * 1024 * 1024
        ),
    )(
        mixer_in, cf, in_real.reshape(FL, 16), in_imag.reshape(FL, 16),
        output_real.reshape(CHD, 64), output_imaginary.reshape(CHD, 64),
        skip.reshape(1, CHD), out_proj, norm_gain.reshape(1, D),
        residual, w_gate, w_up, w_down,
    )


def solution(mesh):
    finer = Mesh(mesh.devices.reshape(NZ, NY, mesh.shape["tp"]), ("sp_0", "sp_1", "tp"))
    return jax.shard_map(
        on_device,
        mesh=finer,
        in_specs=(
            P(SP, "tp"),
            P(SP_TP, None),
            P("tp", None),
            P("tp", None),
            P("tp"),
            P("tp", None, None),
            P("tp", None, None),
            P("tp", None, None),
            P("tp", None, None),
            P("tp"),
            P("tp", None),
            P(),
            P(SP, "tp"),
            P(SP, "tp"),
            P("tp", SP),
        ),
        out_specs=P(SP_TP, None),
        check_vma=False,
    )
```

time: 291 us -> 119 us (0.41)
  blocking collectives: 114 us -> 0 us
  Pallas kernels: 0 us -> 112 us
  waiting for transfers between devices: 83.3 us -> 0 us
  local copies, waits for them, and re-layouts: 27.4 us -> 5.14 us
  starting transfers between devices: 19.3 us -> 0 us
  matrix products: 17.5 us -> 0 us
  between operations: 14.1 us -> 0.02 us
  other arithmetic: 13.5 us -> 1.43 us
    pallas_call x0 -> x1, Pallas kernels: none -> 112 us  [on_device(): pl.pallas_call(kernel, out_shape=jax.ShapeDtypeStruct((ROWS, D), BF16), i...]
    all_to_all x3 -> x0, blocking collectives: 103 us -> none  [the longest x2 73.5 us: sent_and_summed(): lax.all_to_all(cut_along(array, dim, length), axis, 0, 0, tiled=True)]
    all_gather x2 -> x0, waiting for transfers between devices: 78.2 us -> none  [the longest x1 66.9 us: whole_of(): array = lax.all_gather(array, axis, axis=dim, tiled=True)]
    all_to_all x1 -> x0, starting transfers between devices: 19.3 us -> none  [sent_to_all(): return lax.all_to_all(copies, axis, split_axis=0, concat_axis=0, tiled=True)]
    dot_general x5 -> x0, matrix products: 17.5 us -> none  [the longest x1 9.27 us: on_device(): jnp.dot(hidden, whole_down, preferred_element_type=jnp.float32)]
    all_gather x1 -> x0, blocking collectives: 11.4 us -> none  [whole_of(): array = lax.all_gather(array, axis, axis=dim, tiled=True)]
    slice x63 -> x0, local copies, waits for them, and re-layouts: 8.09 us -> none  [the longest x40 6.34 us: joined_by_halves(): part[side::2]]
    add x12 -> x0, local copies, waits for them, and re-layouts: 6.83 us -> none  [the longest x6 4.71 us: local_states(): power_re * cur_re - power_im * cur_im + dr[:, index]]
  transfers between devices with their start and end apart: 3 -> 0, of which waited for: 3 -> 0; matrix products, arithmetic and copies ran while one was open for 16% -> 0% of each run, Pallas kernels for 0% -> 0%
where the time goes in v1:
time: 119 us; the launch traced here: 118 us
  Pallas kernels  112 us (94%)
  local copies, waits for them, and re-layouts  5.14 us (4%)
  other arithmetic  1.43 us (1%)
    pallas_call x1, Pallas kernels, on_device(): pl.pallas_call(kernel, out_shape=jax.ShapeDtypeStruct((ROWS, D), BF16), i...  112 us
    unnamed x10, local copies, waits for them, and re-layouts  4.18 us

profile of v1, /device:TPU:1, one launch (start us, length us, event | category | flops | bytes accessed | tf_op | source)
XLA Modules:
  0.0 118.2 jit_solution(6694987998905867884)
XLA Ops:
  0.0 0.0 copy-start.2
  0.0 0.7 exp.6
  0.7 0.8 cosine_multiply_fusion
  1.5 0.1 stack.15
  1.6 0.1 stack.16
  1.6 0.1 stack.18
  1.7 0.1 stack.17
  1.8 0.6 pad_maximum_fusion.cf_ref
  2.4 0.0 copy-done.2
  2.4 0.0 copy-start
  2.4 0.8 copy.18.wd_ref
  3.2 0.0 copy-done
  3.3 0.0 copy-start.1
  3.3 0.8 copy.16
  4.1 0.0 copy-done.1
  4.1 0.8 copy.17
  4.9 111.6 %shard_map.145 = bf16[64,2048]{1,0:T(8,128)(2,1)} custom-call(bf16[512,128]{1,0:T(8,128)(2,1)} %x_ref.1, f32[4,512]{1,0:T(4,128)} %pad_maximum_fusion.cf_ref, f32[512,16]{1,0:T(8,128)} %bitcast.6, f32[512,16]{1,0:T(8,128)} %bitcast.7, f32[128,64]{1,0:T(8,128)} %bitcast.8, f32[128,64]{1,0:T(8,128)} %bitcast.9, f32[1,128]{1,0:T(1,128)} %bitcast.11, ...), custom_call_target="tpu_custom_call" | custom-call | tf_op jit(solution)/shard_map/pallas_call | solution.py:503
  116.5 1.7 %copy.20 = bf16[64,2048]{1,0:T(8,128)(2,1)} copy(bf16[64,2048]{1,0:T(8,128)(2,1)} %shard_map.145) | data formatting | bytes 524288
Async XLA Ops:
  0.0 2.4 %copy-start.2 = (bf16[704,32]{0,1:T(8,128)(2,1)S(1)}, bf16[704,32]{0,1:T(8,128)(2,1)}, u32[]{:S(2)}) copy-start(bf16[704,32]{0,1:T(8,128)(2,1)} %param.29) | copy-start | bytes 135172
  2.4 0.8 copy-start
  3.3 0.8 copy-start.1

commit v2 on v1

v2 whole, which is shorter than its diff:
```python
import functools

import jax
import jax.numpy as jnp
from jax import lax
from jax.experimental import pallas as pl
from jax.experimental.pallas import tpu as pltpu
from jax.sharding import Mesh
from jax.sharding import PartitionSpec as P

SP = ("sp_0", "sp_1")
SP_TP = ("sp_0", "sp_1", "tp")
MESH = pl.DeviceIdType.MESH
F32 = jnp.float32
BF16 = jnp.bfloat16

NZ = 16
NY = 4
NX = 4
NT = 8
HALF = NZ // 2
D = 2048
TOK = 512
ROWS = TOK // NT
FL = 512
CHD = 128
FFD = 704
GU = 2 * FFD
CA = 512
SPANS = ((0, 3), (3, 6), (6, 7), (7, 8))
NC = len(SPANS)


def discrete(decay_real, decay_imag, log_step):
    step_size = jnp.exp(log_step)
    magnitude = jnp.exp(decay_real * step_size)
    angle = decay_imag * step_size
    power_re = magnitude * jnp.cos(angle)
    power_im = magnitude * jnp.sin(angle)
    denom = decay_real * decay_real + decay_imag * decay_imag
    ratio_re = ((power_re - 1.0) * decay_real + power_im * decay_imag) / denom
    ratio_im = (power_im * decay_real - (power_re - 1.0) * decay_imag) / denom
    return (power_re, power_im), (ratio_re, ratio_im)


def cmul(a, b):
    return (a[0] * b[0] - a[1] * b[1], a[0] * b[1] + a[1] * b[0])


def cadd(a, b):
    return (a[0] + b[0], a[1] + b[1])


def pieces(v):
    hi = v.astype(BF16)
    lo = (v - hi.astype(F32)).astype(BF16)
    return hi, lo


def dot(a, b):
    return jnp.dot(a, b, preferred_element_type=F32)


def dot_t(a, b):
    return lax.dot_general(a, b, (((1,), (1,)), ((), ())), preferred_element_type=F32)


def packed(row):
    return jnp.concatenate([row[:, i * 128 : (i + 1) * 128] for i in range(4)], axis=0)


def flat(block):
    return jnp.concatenate([block[i : i + 1] for i in range(4)], axis=1)


class Phase:
    def __init__(self):
        self.scope = None

    def __call__(self, name):
        if self.scope is not None:
            self.scope.__exit__(None, None, None)
        self.scope = None
        if name:
            self.scope = jax.named_scope(name)
            self.scope.__enter__()


class Ring:
    count = 33

    def __init__(self, net, buf, sems):
        self.net, self.buf = net, buf
        (self.ya_recv, self.ya_send, self.za_recv, self.za_send,
         self.zb_recv, self.zb_send, self.yb_recv, self.yb_send) = sems

    def a_y(self, zb, yb):
        return self.buf.at[zb * NY + yb, :, 0:CA]

    def a_z(self, zb, h):
        return self.buf.at[pl.ds(zb * NY + 2 * h, 2), :, 0:CA]

    def b(self, zb, yb):
        return self.buf.at[zb * NY + yb, :, CA:GU]

    def start_ya(self):
        n = self.net
        blk = self.a_y(n.z, n.y)
        for k in range(1, NY):
            n.send(blk, blk, self.ya_send.at[k], self.ya_recv.at[n.y], sp_1=(n.y + k) % NY)

    def finish_ya(self):
        n = self.net
        for k in range(1, NY):
            yk = (n.y + k) % NY
            n.arrived(self.a_y(n.z, yk), self.ya_send.at[k], self.ya_recv.at[yk], sp_1=yk)

    def forward_a(self, zb, chain, s, h):
        n = self.net
        blk = self.a_z(zb, h)
        n.send(blk, blk, self.za_send.at[(chain * HALF + s) * 2 + h], self.za_recv.at[zb * 2 + h],
               sp_0=n.zp if chain == 0 else n.zm)

    def forward_b(self, zb, chain, s):
        n = self.net
        blk = self.b(zb, n.y)
        n.send(blk, blk, self.zb_send.at[chain * HALF + s], self.zb_recv.at[zb],
               sp_0=n.zp if chain == 0 else n.zm)

    def start_yb(self, zb, o):
        n = self.net
        blk = self.b(zb, n.y)
        sem = self.yb_recv.at[zb * NY + n.y]
        n.send(blk, blk, self.yb_send.at[3 * o], sem, sp_1=n.yp)
        n.send(blk, blk, self.yb_send.at[3 * o + 1], sem, sp_1=n.ym)

    def own_a(self):
        self.finish_ya()
        for h in (0, 1):
            for chain in (0, 1):
                self.forward_a(self.net.z, chain, 0, h)

    def own_bz(self):
        for chain in (0, 1):
            self.forward_b(self.net.z, chain, 0)

    def own_by(self):
        self.start_yb(self.net.z, 0)

    def tick_a(self, s, h):
        n = self.net
        for chain in n.chains(s):
            zb = n.block(chain, s)
            n.arrived(self.a_z(zb, h), self.za_send.at[0], self.za_recv.at[zb * 2 + h], sp_0=n.zm)
            if n.goes_on(chain, s):
                self.forward_a(zb, chain, s, h)

    def tick_b(self, s):
        n = self.net
        for chain in n.chains(s):
            zb = n.block(chain, s)
            n.arrived(self.b(zb, n.y), self.zb_send.at[0], self.zb_recv.at[zb], sp_0=n.zm)
            if n.goes_on(chain, s):
                self.forward_b(zb, chain, s)
            self.start_yb(zb, n.order(chain, s))

    def tick_y(self, s):
        n = self.net
        for chain in n.chains(s):
            zb, o = n.block(chain, s), n.order(chain, s)
            blk = self.b(zb, n.ym)
            sem = self.yb_recv.at[zb * NY + n.ym]
            n.arrived(blk, self.yb_send.at[3 * o + 2], sem, sp_1=n.ym)
            n.send(blk, blk, self.yb_send.at[3 * o + 2], sem, sp_1=n.yp)

    def finish(self, s):
        n = self.net
        for chain in n.chains(s):
            zb, o = n.block(chain, s), n.order(chain, s)
            for yb in (n.yp, n.y2):
                n.arrived(self.b(zb, yb), self.yb_send.at[3 * o],
                          self.yb_recv.at[zb * NY + yb], sp_1=n.yp)


RING_SEMS = [NY, NY, 2 * NZ, 4 * HALF, NZ, NZ, NZ * NY, 3 * NZ]


class Pool:
    def __init__(self, net, buf, recv, ssem):
        self.net, self.buf, self.recv, self.ssem = net, buf, recv, ssem

    def at(self, b, h):
        return self.buf.at[b, :, h * (D // 2) : (h + 1) * (D // 2)]

    def put(self, b, h, k, to):
        blk = self.at(b, h)
        self.net.send(blk, blk, self.ssem.at[2 * k + h], self.recv.at[b * 2 + h], tp=to)

    def get(self, b, h, frm):
        self.net.arrived(self.at(b, h), self.ssem.at[0], self.recv.at[b * 2 + h], tp=frm)

    def start(self, h):
        n = self.net
        self.put(n.t, h, 0, n.tpp)
        self.put(n.t, h, 1, n.tpm)
        self.put(n.t, h, 2, n.tpo)

    def forward(self, h):
        n = self.net
        self.get(n.tpm, h, n.tpm)
        self.put(n.tpm, h, 3, n.tpp)
        self.put(n.tpm, h, 4, n.tpo)
        self.get(n.tpp, h, n.tpp)
        self.put(n.tpp, h, 5, n.tpo)

    def last(self, h):
        n = self.net
        self.get(n.tp2, h, n.tpm)
        self.put(n.tp2, h, 6, n.tpo)

    def finish(self, h):
        n = self.net
        for xb in (n.x, n.xp, n.xm, n.x2):
            self.get(xb * 2 + n.other, h, n.tpo)


class Net:
    def __init__(self):
        self.z = lax.axis_index("sp_0")
        self.y = lax.axis_index("sp_1")
        self.t = lax.axis_index("tp")
        z, y, t = self.z, self.y, self.t
        x, c = t // 2, t % 2
        self.x, self.c = x, c
        self.yp = (y + 1 + 2 * c) % NY
        self.ym = (y + 3 + 2 * c) % NY
        self.y2 = (y + 2) % NY
        self.zp = (z + 1 + (NZ - 2) * c) % NZ
        self.zm = (z + NZ - 1 + 2 * c) % NZ
        self.xp = (x + 1 + 2 * c) % NX
        self.xm = (x + 3 + 2 * c) % NX
        self.x2 = (x + 2) % NX
        self.other = 1 - c
        self.tpp = self.xp * 2 + c
        self.tpm = self.xm * 2 + c
        self.tp2 = self.x2 * 2 + c
        self.tpo = x * 2 + self.other
        self.sent = []

    def copy(self, src, dst, ss, rs, **dev):
        return pltpu.make_async_remote_copy(
            src_ref=src, dst_ref=dst, send_sem=ss, recv_sem=rs, device_id=dev, device_id_type=MESH
        )

    def send(self, src, dst, ss, rs, **dev):
        cp = self.copy(src, dst, ss, rs, **dev)
        cp.start()
        self.sent.append(cp)

    def arrived(self, dst, ss, rs, **dev):
        self.copy(dst, dst, ss, rs, **dev).wait_recv()

    def chains(self, s):
        return (0,) if s in (0, HALF) else (0, 1)

    def goes_on(self, chain, s):
        return s < (HALF if chain == 0 else HALF - 1)

    def block(self, chain, s):
        toward = self.zm - self.z if chain == 0 else self.zp - self.z
        return (self.z + NZ * NZ + s * toward) % NZ

    def order(self, chain, s):
        return 0 if s == 0 else 2 * s - 1 + chain


def kernel(
    x_ref, dr_ref, di_ref, ls_ref, inr_ref, ini_ref, our_ref, oui_ref, skip_ref, op_ref, gain_ref,
    res_ref, wg_ref, wu_ref, wd_ref, out_ref,
    wgu, wdn, opall, sb, tb, act, acts, nf, hid, part, pr, ps, rs,
    ur, ui, mr, mi, er, ei, pcr, pci, carried, *sems,
):
    net = Net()
    phase = Phase()
    z, y, t = net.z, net.y, net.t
    send, arrived = net.send, net.arrived
    gu = Ring(net, wgu, sems[0:8])
    dn = Ring(net, wdn, sems[8:16])
    (o_recv, o_send, n_recv, n_send, s_recv, s_send, t_recv, t_send, a_recv, a_send,
     p_recv, p_send, r_recv, r_send) = sems[16:]
    oproj = Pool(net, opall, o_recv, o_send)
    norms = Pool(net, nf, n_recv, n_send)

    phase("signal")
    barrier = pltpu.get_barrier_semaphore()
    for k in range(1, NZ):
        pl.semaphore_signal(barrier, inc=1, device_id={"sp_0": (z + k) % NZ}, device_id_type=MESH)
    for k in range(1, NY):
        pl.semaphore_signal(barrier, inc=1, device_id={"sp_1": (y + k) % NY}, device_id_type=MESH)
    for k in range(1, NT):
        pl.semaphore_signal(barrier, inc=1, device_id={"tp": (t + k) % NT}, device_id_type=MESH)

    phase("own")
    own = z * NY + y
    wgu[own, :, 0:640] = wg_ref[:, 0:640]
    wgu[own, :, 640:1280] = wu_ref[:, 0:640]
    wgu[own, :, 1280:1408] = jnp.concatenate([wg_ref[:, 640:704], wu_ref[:, 640:704]], axis=1)
    wdn[own, :, 0:640] = wd_ref[0:16, 0:640]
    wdn[own, :, 640:1280] = wd_ref[16:32, 0:640]
    wdn[own, :, 1280:1408] = jnp.concatenate([wd_ref[0:16, 640:704], wd_ref[16:32, 640:704]], axis=1)
    opall[t] = op_ref[...]

    phase("coef")
    eight = lax.broadcasted_iota(jnp.int32, (8, 8), 0) == lax.broadcasted_iota(jnp.int32, (8, 8), 1)
    log_step = jnp.sum(
        jnp.where(eight, jnp.broadcast_to(ls_ref[...], (8, 8)), 0.0), axis=1, keepdims=True
    )
    a, ratio = discrete(dr_ref[...], di_ref[...], log_step)

    def line(v):
        return jnp.concatenate([v[g : g + 1] for g in range(8)], axis=1)

    a = (line(a[0]), line(a[1]))
    ratio = (line(ratio[0]), line(ratio[1]))
    powers = [a]
    for _ in range(7):
        powers.append(cmul(powers[-1], a))
    lift = tuple(jnp.concatenate([p[i] for p in powers], axis=0) for i in (0, 1))
    row8 = lax.broadcasted_iota(jnp.int32, (8, FL), 0)
    masked = []
    for k in (1, 2, 4):
        p = powers[k - 1]
        masked.append(tuple(jnp.where(row8 >= k, jnp.broadcast_to(v, (8, FL)), 0.0) for v in p))

    phase("drive")
    spread = (
        lax.broadcasted_iota(jnp.int32, (64, FL), 1) % 64
        == lax.broadcasted_iota(jnp.int32, (64, FL), 0)
    ).astype(F32).astype(BF16)
    block = (
        lax.broadcasted_iota(jnp.int32, (CHD, FL), 0) // 16
        == lax.broadcasted_iota(jnp.int32, (CHD, FL), 1) // 64
    )
    signal = x_ref[...]
    for src, dst in ((inr_ref, ur), (ini_ref, ui)):
        total = None
        for piece in pieces(src[...]):
            wide = jnp.where(block, dot(piece, spread), 0.0).astype(BF16)
            term = dot(signal, wide)
            total = term if total is None else total + term
        dst[...] = total

    phase("barrier")
    pl.semaphore_wait(barrier, NT - 1 + NY - 1 + NZ - 1)

    phase("first_sends")
    gu.start_ya()
    gu.own_bz()
    gu.own_by()
    oproj.start(0)
    oproj.start(1)
    dn.own_bz()

    phase("scan")

    def tile_step(i, carry):
        for j in range(4):
            rows = pl.ds(pl.multiple_of(i * 32 + j * 8, 8), 8)
            v = cmul(ratio, (ur[rows, :], ui[rows, :]))
            for k, m in zip((1, 2, 4), masked):
                v = cadd(v, cmul(m, (pltpu.roll(v[0], k, 0), pltpu.roll(v[1], k, 0))))
            ur[rows, :] = v[0]
            ui[rows, :] = v[1]
            er[pl.ds(i * 4 + j, 1), :] = v[0][7:8]
            ei[pl.ds(i * 4 + j, 1), :] = v[1][7:8]
        return carry

    lax.fori_loop(0, TOK // 32, tile_step, 0)

    phase("ends")
    row64 = lax.broadcasted_iota(jnp.int32, (64, FL), 0)
    e = (er[...], ei[...])
    ladder = []
    p = powers[7]
    for k in (1, 2, 4, 8, 16, 32):
        ladder.append(p)
        moved = tuple(jnp.where(row64 >= k, pltpu.roll(v, k, 0), 0.0) for v in e)
        e = cadd(e, cmul(p, moved))
        p = cmul(p, p)
    er[...] = e[0]
    ei[...] = e[1]
    a512 = (packed(p[0]), packed(p[1]))
    last = (e[0][63:64], e[1][63:64])
    sb[y, 0:4, :] = packed(last[0])
    sb[y, 4:8, :] = packed(last[1])
    for k in range(1, NY):
        send(sb.at[y], sb.at[y], s_send.at[k], s_recv.at[y], sp_1=(y + k) % NY)
    dn.start_ya()

    phase("lead")
    lead = (jnp.ones((64, FL), F32), jnp.zeros((64, FL), F32))
    for b, q in enumerate(ladder):
        more = cmul(q, lead)
        bit = (row64 // (1 << b)) % 2 == 1
        lead = tuple(jnp.where(bit, m, v) for m, v in zip(more, lead))
    pcr[...] = lead[0]
    pci[...] = lead[1]

    phase("outmat")
    for k, (src, sign) in enumerate(((our_ref, 1.0), (oui_ref, -1.0))):
        hi, lo = pieces(src[...] * sign)
        mr[k] = jnp.where(block, dot(hi, spread), 0.0).astype(BF16)
        mi[k] = jnp.where(block, dot(lo, spread), 0.0).astype(BF16)

    phase("s_wait")
    for k in range(1, NY):
        yk = (y + k) % NY
        arrived(sb.at[yk], s_send.at[k], s_recv.at[yk], sp_1=yk)
    whole = (jnp.zeros((4, 128), F32), jnp.zeros((4, 128), F32))
    before = whole
    ahead = (jnp.ones((4, 128), F32), jnp.zeros((4, 128), F32))
    for b in range(NY):
        own_b = (sb[b, 0:4, :], sb[b, 4:8, :])
        whole = cadd(cmul(a512, whole), own_b)
        inside = b < y
        step_b = cadd(cmul(a512, before), own_b)
        before = tuple(jnp.where(inside, n, v) for n, v in zip(step_b, before))
        step_a = cmul(a512, ahead)
        ahead = tuple(jnp.where(inside, n, v) for n, v in zip(step_a, ahead))
    a2 = cmul(a512, a512)
    a4 = cmul(a2, a2)
    tb[z, 0:4, :] = whole[0]
    tb[z, 4:8, :] = whole[1]
    for k in range(1, NZ):
        send(tb.at[z], tb.at[z], t_send.at[k], t_recv.at[z], sp_0=(z + k) % NZ)

    phase("b1")
    gu.tick_b(1)
    phase("own_a")
    gu.own_a()
    phase("b2")
    gu.tick_y(0)
    gu.tick_b(2)
    phase("op0")
    oproj.forward(0)
    phase("y1")
    gu.tick_y(1)
    dn.tick_b(1)
    phase("a1")
    gu.tick_a(1, 0)
    gu.tick_a(1, 1)
    phase("b3")
    gu.tick_b(3)
    gu.tick_y(2)

    phase("t_wait")
    for k in range(1, NZ):
        zk = (z + k) % NZ
        arrived(tb.at[zk], t_send.at[k], t_recv.at[zk], sp_0=zk)
    phase("hold")
    hold = (jnp.zeros((4, 128), F32), jnp.zeros((4, 128), F32))
    for b in range(NZ - 1):
        step_h = cadd(cmul(a4, hold), (tb[b, 0:4, :], tb[b, 4:8, :]))
        hold = tuple(jnp.where(b < z, n, v) for n, v in zip(step_h, hold))
    hold = cadd(cmul(ahead, hold), before)
    hold = (flat(hold[0]), flat(hold[1]))
    enter = cmul((pcr[...], pci[...]), hold)
    prev = tuple(jnp.where(row64 >= 1, pltpu.roll(v[...], 1, 0), 0.0) for v in (er, ei))
    enter = cadd(enter, prev)
    pcr[...] = enter[0]
    pci[...] = enter[1]

    phase("read")

    def read_step(i, carry):
        re, im = [], []
        for j in range(16):
            k = i * 16 + j
            rows = pl.ds(pl.multiple_of(k * 8, 8), 8)
            w = (pcr[pl.ds(k, 1), :], pci[pl.ds(k, 1), :])
            v = cadd((ur[rows, :], ui[rows, :]), cmul(lift, w))
            re.append(v[0])
            im.append(v[1])
        total = None
        for k, v in enumerate((re, im)):
            hi, lo = pieces(jnp.concatenate(v, axis=0))
            term = dot_t(hi, mr[k]) + dot_t(hi, mi[k]) + dot_t(lo, mr[k])
            total = term if total is None else total + term
        rows = pl.ds(pl.multiple_of(i * 128, 128), 128)
        pre = total + skip_ref[...] * x_ref[rows, :].astype(F32)
        inner = 0.7978845608028654 * (pre + 0.044715 * (pre * pre * pre))
        val = (pre * (0.5 * (1.0 + jnp.tanh(inner)))).astype(BF16)
        act[2 * i] = val[0:64]
        act[2 * i + 1] = val[64:128]
        return carry

    lax.fori_loop(0, 4, read_step, 0)
    for k in range(1, NT):
        tk = (t + k) % NT
        send(act.at[tk], acts.at[t], a_send.at[k], a_recv.at[t], tp=tk)
    acts[t] = act[t]

    phase("op1")
    oproj.forward(1)
    phase("a2")
    gu.tick_a(2, 0)
    gu.tick_a(2, 1)
    phase("b4")
    gu.tick_b(4)
    gu.tick_y(3)
    oproj.last(0)
    phase("a3")
    gu.tick_a(3, 0)
    gu.tick_a(3, 1)
    dn.own_a()
    dn.own_by()
    phase("op_fin")
    oproj.last(1)
    oproj.finish(0)
    oproj.finish(1)

    phase("a_wait")
    for k in range(1, NT):
        tk = (t + k) % NT
        arrived(acts.at[tk], a_send.at[k], a_recv.at[tk], tp=tk)

    phase("mix")

    def mix_step(j, squares):
        cols = pl.ds(pl.multiple_of(j * 256, 256), 256)
        total = jnp.zeros((ROWS, 256), F32)
        for b in range(NT):
            total = total + dot(acts[b], opall[b, :, cols]).astype(BF16).astype(F32)
        v = res_ref[:, cols].astype(F32) + total.astype(BF16).astype(F32)
        carried[:, cols] = v
        return squares + jnp.sum(v * v, axis=1, keepdims=True)

    squares = lax.fori_loop(0, D // 512, mix_step, jnp.zeros((ROWS, 1), F32))
    gu.tick_b(5)
    gu.tick_y(4)
    squares = lax.fori_loop(D // 512, D // 256, mix_step, squares)
    scale = lax.rsqrt(squares * (1.0 / D) + 1e-06)
    nf[t] = (carried[...] * scale * gain_ref[...]).astype(BF16)
    norms.start(0)
    norms.start(1)
    phase("a4")
    gu.tick_a(4, 0)
    gu.tick_a(4, 1)
    dn.tick_b(2)
    phase("b6")
    gu.tick_b(6)
    gu.tick_y(5)
    phase("a5")
    gu.tick_a(5, 0)
    dn.tick_a(1, 0)
    gu.tick_a(5, 1)
    dn.tick_a(1, 1)
    phase("n0")
    norms.forward(0)
    phase("b7")
    gu.tick_b(7)
    gu.tick_y(6)
    dn.tick_b(3)
    dn.tick_y(0)
    phase("a6")
    gu.tick_a(6, 0)
    dn.tick_a(2, 0)
    gu.tick_a(6, 1)
    dn.tick_a(2, 1)
    phase("n1")
    norms.forward(1)
    norms.last(0)
    phase("b8")
    gu.tick_b(8)
    gu.tick_y(7)
    dn.tick_b(4)
    dn.tick_y(1)
    phase("a7")
    gu.tick_a(7, 0)
    dn.tick_a(3, 0)
    gu.tick_a(7, 1)
    dn.tick_a(3, 1)
    norms.last(1)
    gu.tick_y(8)
    dn.tick_y(2)
    phase("b5d")
    dn.tick_b(5)
    phase("a8")
    gu.tick_a(8, 0)
    dn.tick_a(4, 0)
    gu.tick_a(8, 1)
    dn.tick_a(4, 1)
    dn.tick_y(3)
    phase("n_fin")
    norms.finish(0)
    norms.finish(1)
    phase("g_fin")
    for s in range(0, HALF + 1):
        gu.finish(s)

    def up_step(j):
        w = jnp.concatenate(
            [wgu[:, :, j * 128 : (j + 1) * 128].reshape(D, 128),
             wgu[:, :, 640 + j * 128 : 768 + j * 128].reshape(D, 128)], axis=1
        )
        v = dot(nf[...].reshape(TOK, D), w)
        g = v[:, 0:128]
        hid[:, j * 128 : (j + 1) * 128] = (g / (1.0 + jnp.exp(-g)) * v[:, 128:256]).astype(BF16)

    phase("up0")
    up_step(0)
    up_step(1)
    phase("d5")
    dn.tick_b(6)
    dn.tick_y(4)
    dn.tick_a(5, 0)
    dn.tick_a(5, 1)
    dn.tick_y(5)
    phase("up1")
    up_step(2)
    up_step(3)
    phase("d6")
    dn.tick_b(7)
    dn.tick_a(6, 0)
    dn.tick_a(6, 1)
    dn.tick_y(6)
    phase("up2")
    up_step(4)
    v = dot(nf[...].reshape(TOK, D), wgu[:, :, 1280:1408].reshape(D, 128))
    v = v / (1.0 + jnp.exp(-v)) * pltpu.roll(v, 64, 1)
    low = lax.broadcasted_iota(jnp.int32, (TOK, 128), 1) < 64
    hid[:, 640:768] = jnp.where(low, v, 0.0).astype(BF16)

    def weights_of(zb):
        v = wdn[pl.ds(zb * NY, NY)]
        main = jnp.concatenate([v[:, :, 0:640], v[:, :, 640:1280]], axis=1).reshape(128, 640)
        tail = v[:, :, 1280:1408]
        turned = pltpu.roll(tail.reshape(64, 128).astype(F32), 64, 1).astype(BF16)
        tail = jnp.concatenate([tail, turned.reshape(NY, 16, 128)], axis=1).reshape(128, 128)
        return jnp.concatenate([main, tail], axis=1)

    def place(o):
        s = o // 2 + 1
        if s == HALF:
            return (z + HALF * (o % 2)) % NZ
        return (z + (s if o % 2 else NZ - s)) % NZ

    def down_step(i):
        w = jnp.concatenate([weights_of(place(2 * i)), weights_of(place(2 * i + 1))], axis=0)
        v = dot_t(hid[...], w)
        part[:, :, i * 256 : (i + 1) * 256] = v.astype(BF16).reshape(NT, ROWS, 256)

    xs = (net.x2, net.xm, net.xp, net.x)

    def span(k):
        return pl.ds(SPANS[k][0] * 256, (SPANS[k][1] - SPANS[k][0]) * 256)

    def sum_start(k):
        for i, xb in enumerate(xs):
            send(part.at[xb * 2 + net.other, :, span(k)], pr.at[xb, :, span(k)],
                 p_send.at[4 * k + i], p_recv.at[NX * k + xb], tp=net.tpo)

    def pair(k, xb):
        arrived(pr.at[xb, :, span(k)], p_send.at[0], p_recv.at[NX * k + xb], tp=net.tpo)
        mine = part[xb * 2 + net.c, :, span(k)].astype(F32)
        return mine + pr[xb, :, span(k)].astype(F32)

    def sum_pair(k):
        for i, (xb, to) in enumerate(((net.x2, net.tp2), (net.xm, net.tpm), (net.xp, net.tpp))):
            ps[i, :, span(k)] = pair(k, xb).astype(BF16)
            send(ps.at[i, :, span(k)], rs.at[i, :, span(k)],
                 r_send.at[3 * k + i], r_recv.at[3 * k + i], tp=to)

    def sum_finish(k):
        total = pair(k, net.x)
        for i, frm in enumerate((net.tp2, net.tpp, net.tpm)):
            arrived(rs.at[i, :, span(k)], r_send.at[0], r_recv.at[3 * k + i], tp=frm)
            total = total + rs[i, :, span(k)].astype(F32)
        total = total.astype(BF16).astype(F32)
        for i in range(2 * (SPANS[k][1] - SPANS[k][0])):
            cols = pl.ds(pl.multiple_of(place(2 * SPANS[k][0] + i) * 128, 128), 128)
            v = carried[:, cols] + 0.5 * total[:, i * 128 : (i + 1) * 128]
            out_ref[:, cols] = v.astype(BF16)

    phase("w0")
    dn.tick_b(8)
    dn.finish(1)
    down_step(0)
    dn.finish(2)
    down_step(1)
    phase("d7")
    dn.tick_a(7, 0)
    dn.tick_a(7, 1)
    dn.tick_y(7)
    dn.tick_y(8)
    phase("w2")
    dn.finish(3)
    down_step(2)
    sum_start(0)
    dn.finish(4)
    down_step(3)
    phase("w4")
    sum_pair(0)
    dn.finish(5)
    down_step(4)
    phase("w5")
    dn.finish(6)
    down_step(5)
    sum_start(1)
    phase("w6")
    dn.finish(7)
    down_step(6)
    sum_start(2)
    sum_pair(1)
    phase("d8")
    dn.tick_a(8, 0)
    dn.tick_a(8, 1)
    dn.finish(0)
    dn.finish(8)
    phase("w7")
    down_step(7)
    sum_start(3)
    phase("rs")
    sum_finish(0)
    sum_pair(2)
    sum_pair(3)
    sum_finish(1)
    sum_finish(2)
    sum_finish(3)

    phase("drain")
    for cp in net.sent:
        cp.wait_send()
    phase(None)


def on_device(
    mixer_in, residual, decay_real, decay_imag, log_step, in_real, in_imag,
    output_real, output_imaginary, skip, out_proj, norm_gain, w_gate, w_up, w_down,
):
    vmem = pltpu.VMEM
    dma = pltpu.SemaphoreType.DMA
    scratch = [
        vmem((NZ * NY, 32, GU), BF16),
        vmem((NZ * NY, 16, GU), BF16),
        vmem((NT, CHD, D), BF16),
        vmem((NY, 8, 128), F32),
        vmem((NZ, 8, 128), F32),
        vmem((NT, ROWS, CHD), BF16),
        vmem((NT, ROWS, CHD), BF16),
        vmem((NT, ROWS, D), BF16),
        vmem((TOK, 768), BF16),
        vmem((NT, ROWS, D), BF16),
        vmem((NX, ROWS, D), BF16),
        vmem((3, ROWS, D), BF16),
        vmem((3, ROWS, D), BF16),
        vmem((TOK, FL), F32),
        vmem((TOK, FL), F32),
        vmem((2, CHD, FL), BF16),
        vmem((2, CHD, FL), BF16),
        vmem((64, FL), F32),
        vmem((64, FL), F32),
        vmem((64, FL), F32),
        vmem((64, FL), F32),
        vmem((ROWS, D), F32),
    ]
    counts = RING_SEMS + RING_SEMS + [
        2 * NT, 14, 2 * NT, 14, NY, NY, NZ, NZ, NT, NT, NC * NX, NC * 4, NC * 3, NC * 3,
    ]
    scratch += [dma((n,)) for n in counts]
    return pl.pallas_call(
        kernel,
        out_shape=jax.ShapeDtypeStruct((ROWS, D), BF16),
        in_specs=[pl.BlockSpec(memory_space=vmem)] * 15,
        out_specs=pl.BlockSpec(memory_space=vmem),
        scratch_shapes=scratch,
        compiler_params=pltpu.CompilerParams(
            collective_id=0, has_side_effects=True, vmem_limit_bytes=60 * 1024 * 1024
        ),
    )(
        mixer_in, decay_real, decay_imag, log_step.reshape(1, 8),
        jnp.transpose(in_real, (0, 2, 1)).reshape(CHD, 64),
        jnp.transpose(in_imag, (0, 2, 1)).reshape(CHD, 64),
        output_real.reshape(CHD, 64), output_imaginary.reshape(CHD, 64),
        skip.reshape(1, CHD), out_proj, norm_gain.reshape(1, D),
        residual, w_gate, w_up, w_down.T,
    )


def solution(mesh):
    finer = Mesh(mesh.devices.reshape(NZ, NY, mesh.shape["tp"]), ("sp_0", "sp_1", "tp"))
    return jax.shard_map(
        on_device,
        mesh=finer,
        in_specs=(
            P(SP, "tp"),
            P(SP_TP, None),
            P("tp", None),
            P("tp", None),
            P("tp"),
            P("tp", None, None),
            P("tp", None, None),
            P("tp", None, None),
            P("tp", None, None),
            P("tp"),
            P("tp", None),
            P(),
            P(SP, "tp"),
            P(SP, "tp"),
            P("tp", SP),
        ),
        out_specs=P(SP_TP, None),
        check_vma=False,
    )
```

time: 119 us -> 102 us (0.86)
  Pallas kernels: 112 us -> 99.8 us
  local copies, waits for them, and re-layouts: 5.14 us -> 1.67 us
  other arithmetic: 1.43 us -> 0 us
    pallas_call x1, Pallas kernels: 112 us -> 99.8 us  [on_device(): pl.pallas_call(kernel, out_shape=jax.ShapeDtypeStruct((ROWS, D), BF16), i...]
    unnamed x10 -> x1, local copies, waits for them, and re-layouts: 4.18 us -> 1.67 us
where the time goes in v2:
time: 102 us; the launch traced here: 101 us
  Pallas kernels  99.8 us (98%)
  local copies, waits for them, and re-layouts  1.67 us (2%)
    pallas_call x1, Pallas kernels, on_device(): pl.pallas_call(kernel, out_shape=jax.ShapeDtypeStruct((ROWS, D), BF16), i...  99.8 us

profile of v2, /device:TPU:1, one launch (start us, length us, event | category | flops | bytes accessed | tf_op | source)
XLA Modules:
  0.0 101.5 jit_solution(4648545922032425549)
XLA Ops:
  0.0 99.8 %shard_map.145 = bf16[64,2048]{1,0:T(8,128)(2,1)} custom-call(bf16[512,128]{1,0:T(8,128)(2,1)} %x_ref.1, f32[8,64]{1,0:T(8,128)} %dr_ref.1, f32[8,64]{1,0:T(8,128)} %di_ref.1, f32[1,8]{1,0:T(1,128)} %bitcast.18, f32[128,64]{1,0:T(8,128)} %bitcast.12, f32[128,64]{1,0:T(8,128)} %bitcast.13, f32[128,64]{1,0:T(8,128)} %bitcast.14, f32[128,64]{1,0:T(8,128)} %bitcast.15, ...), custom_call_target="tpu_custom_call" | custom-call | tf_op jit(solution)/shard_map/pallas_call | solution.py:771
  99.8 1.7 %copy.17 = bf16[64,2048]{1,0:T(8,128)(2,1)} copy(bf16[64,2048]{1,0:T(8,128)(2,1)} %shard_map.145) | data formatting | bytes 524288

commit v3 on v2

--- a/solution.py
+++ b/solution.py
@@ -19,6 +19,7 @@
 NX = 4
 NT = 8
 HALF = NZ // 2
+EARLY = 12
 D = 2048
 TOK = 512
 ROWS = TOK // NT
@@ -27,7 +28,7 @@
 FFD = 704
 GU = 2 * FFD
 CA = 512
-SPANS = ((0, 3), (3, 6), (6, 7), (7, 8))
+SPANS = ((0, 2), (2, 4), (4, 6), (6, 8))
 NC = len(SPANS)
 
 
@@ -278,7 +279,7 @@
     x_ref, dr_ref, di_ref, ls_ref, inr_ref, ini_ref, our_ref, oui_ref, skip_ref, op_ref, gain_ref,
     res_ref, wg_ref, wu_ref, wd_ref, out_ref,
     wgu, wdn, opall, sb, tb, act, acts, nf, hid, part, pr, ps, rs,
-    ur, ui, mr, mi, er, ei, pcr, pci, carried, *sems,
+    ur, ui, mr, mi, er, ei, pcr, pci, carried, acc, *sems,
 ):
     net = Net()
     phase = Phase()
@@ -350,17 +351,6 @@
             total = term if total is None else total + term
         dst[...] = total
 
-    phase("barrier")
-    pl.semaphore_wait(barrier, NT - 1 + NY - 1 + NZ - 1)
-
-    phase("first_sends")
-    gu.start_ya()
-    gu.own_bz()
-    gu.own_by()
-    oproj.start(0)
-    oproj.start(1)
-    dn.own_bz()
-
     phase("scan")
 
     def tile_step(i, carry):
@@ -393,10 +383,6 @@
     last = (e[0][63:64], e[1][63:64])
     sb[y, 0:4, :] = packed(last[0])
     sb[y, 4:8, :] = packed(last[1])
-    for k in range(1, NY):
-        send(sb.at[y], sb.at[y], s_send.at[k], s_recv.at[y], sp_1=(y + k) % NY)
-    dn.start_ya()
-
     phase("lead")
     lead = (jnp.ones((64, FL), F32), jnp.zeros((64, FL), F32))
     for b, q in enumerate(ladder):
@@ -412,6 +398,20 @@
         mr[k] = jnp.where(block, dot(hi, spread), 0.0).astype(BF16)
         mi[k] = jnp.where(block, dot(lo, spread), 0.0).astype(BF16)
 
+    phase("barrier")
+    pl.semaphore_wait(barrier, NT - 1 + NY - 1 + NZ - 1)
+
+    phase("first_sends")
+    for k in range(1, NY):
+        send(sb.at[y], sb.at[y], s_send.at[k], s_recv.at[y], sp_1=(y + k) % NY)
+    gu.own_bz()
+    gu.start_ya()
+    oproj.start(0)
+    oproj.start(1)
+    gu.own_by()
+
+    phase("b1")
+    gu.tick_b(1)
     phase("s_wait")
     for k in range(1, NY):
         yk = (y + k) % NY
@@ -432,31 +432,38 @@
     tb[z, 0:4, :] = whole[0]
     tb[z, 4:8, :] = whole[1]
     for k in range(1, NZ):
-        send(tb.at[z], tb.at[z], t_send.at[k], t_recv.at[z], sp_0=(z + k) % NZ)
-
-    phase("b1")
-    gu.tick_b(1)
+        cp = net.copy(tb.at[z], tb.at[z], t_send.at[k], t_recv.at[z], sp_0=(z + k) % NZ)
+
+        @pl.when(z + k < NZ)
+        def _():
+            cp.start()
+
+
     phase("own_a")
     gu.own_a()
     phase("b2")
+    gu.tick_b(2)
     gu.tick_y(0)
-    gu.tick_b(2)
+    phase("a1")
+    gu.tick_a(1, 0)
     phase("op0")
     oproj.forward(0)
-    phase("y1")
-    gu.tick_y(1)
-    dn.tick_b(1)
-    phase("a1")
-    gu.tick_a(1, 0)
+    phase("a1b")
     gu.tick_a(1, 1)
     phase("b3")
     gu.tick_b(3)
-    gu.tick_y(2)
+    gu.tick_y(1)
+
+    phase("op1")
+    oproj.forward(1)
 
     phase("t_wait")
-    for k in range(1, NZ):
-        zk = (z + k) % NZ
-        arrived(tb.at[zk], t_send.at[k], t_recv.at[zk], sp_0=zk)
+    for b in range(NZ - 1):
+
+        @pl.when(b < z)
+        def _():
+            arrived(tb.at[b], t_send.at[1], t_recv.at[b], sp_0=b)
+
     phase("hold")
     hold = (jnp.zeros((4, 128), F32), jnp.zeros((4, 128), F32))
     for b in range(NZ - 1):
@@ -500,22 +507,25 @@
         send(act.at[tk], acts.at[t], a_send.at[k], a_recv.at[t], tp=tk)
     acts[t] = act[t]
 
-    phase("op1")
-    oproj.forward(1)
     phase("a2")
     gu.tick_a(2, 0)
     gu.tick_a(2, 1)
     phase("b4")
     gu.tick_b(4)
-    gu.tick_y(3)
-    oproj.last(0)
+    phase("y2")
+    gu.tick_y(2)
+    dn.start_ya()
     phase("a3")
     gu.tick_a(3, 0)
+    dn.own_bz()
     gu.tick_a(3, 1)
-    dn.own_a()
-    dn.own_by()
+    phase("op_last")
+    oproj.last(0)
+    oproj.last(1)
+    phase("b5")
+    gu.tick_b(5)
+    gu.tick_y(3)
     phase("op_fin")
-    oproj.last(1)
     oproj.finish(0)
     oproj.finish(1)
 
@@ -523,6 +533,26 @@
     for k in range(1, NT):
         tk = (t + k) % NT
         arrived(acts.at[tk], a_send.at[k], a_recv.at[tk], tp=tk)
+
+    def near(o):
+        s = (o + 1) // 2
+        return (z + (NZ - s if o % 2 else s)) % NZ
+
+    def up_dot(lo, hi, *cols):
+        parts = []
+        for c in cols:
+            blocks = [wgu[pl.ds(near(o) * NY, NY), :, c : c + 128].reshape(128, 128) for o in range(lo, hi)]
+            parts.append(jnp.concatenate(blocks, axis=0))
+        w = parts[0] if len(parts) == 1 else jnp.concatenate(parts, axis=1)
+        return dot(nf[:, :, lo * 128 : hi * 128].reshape(TOK, (hi - lo) * 128), w)
+
+    def up_early(j):
+        acc[:, j * 256 : (j + 1) * 256] = up_dot(0, EARLY, j * 128, 640 + j * 128)
+
+    def up_step(j):
+        v = acc[:, j * 256 : (j + 1) * 256] + up_dot(EARLY, NZ, j * 128, 640 + j * 128)
+        g = v[:, 0:128]
+        hid[:, j * 128 : (j + 1) * 128] = (g / (1.0 + jnp.exp(-g)) * v[:, 128:256]).astype(BF16)
 
     phase("mix")
 
@@ -536,97 +566,96 @@
         return squares + jnp.sum(v * v, axis=1, keepdims=True)
 
     squares = lax.fori_loop(0, D // 512, mix_step, jnp.zeros((ROWS, 1), F32))
-    gu.tick_b(5)
-    gu.tick_y(4)
+    gu.tick_a(4, 0)
+    gu.tick_a(4, 1)
+    dn.own_a()
     squares = lax.fori_loop(D // 512, D // 256, mix_step, squares)
     scale = lax.rsqrt(squares * (1.0 / D) + 1e-06)
-    nf[t] = (carried[...] * scale * gain_ref[...]).astype(BF16)
+    for o in range(NZ):
+        src = pl.ds(pl.multiple_of(near(o) * 128, 128), 128)
+        nf[t, :, o * 128 : (o + 1) * 128] = (carried[:, src] * scale * gain_ref[:, src]).astype(BF16)
     norms.start(0)
     norms.start(1)
-    phase("a4")
-    gu.tick_a(4, 0)
-    gu.tick_a(4, 1)
-    dn.tick_b(2)
     phase("b6")
     gu.tick_b(6)
-    gu.tick_y(5)
+    gu.tick_y(4)
+    dn.tick_b(1)
+    dn.own_by()
     phase("a5")
     gu.tick_a(5, 0)
+    gu.tick_a(5, 1)
     dn.tick_a(1, 0)
-    gu.tick_a(5, 1)
-    dn.tick_a(1, 1)
     phase("n0")
     norms.forward(0)
     phase("b7")
+    dn.tick_a(1, 1)
     gu.tick_b(7)
-    gu.tick_y(6)
-    dn.tick_b(3)
-    dn.tick_y(0)
+    gu.tick_y(5)
+    dn.tick_b(2)
+    phase("n1")
+    norms.forward(1)
     phase("a6")
     gu.tick_a(6, 0)
     dn.tick_a(2, 0)
     gu.tick_a(6, 1)
     dn.tick_a(2, 1)
-    phase("n1")
-    norms.forward(1)
     norms.last(0)
     phase("b8")
     gu.tick_b(8)
-    gu.tick_y(7)
-    dn.tick_b(4)
-    dn.tick_y(1)
+    gu.tick_y(6)
+    dn.tick_b(3)
+    dn.tick_y(0)
+    norms.last(1)
     phase("a7")
     gu.tick_a(7, 0)
     dn.tick_a(3, 0)
     gu.tick_a(7, 1)
     dn.tick_a(3, 1)
-    norms.last(1)
-    gu.tick_y(8)
-    dn.tick_y(2)
-    phase("b5d")
-    dn.tick_b(5)
-    phase("a8")
-    gu.tick_a(8, 0)
-    dn.tick_a(4, 0)
-    gu.tick_a(8, 1)
-    dn.tick_a(4, 1)
-    dn.tick_y(3)
+    gu.tick_y(7)
+    dn.tick_b(4)
+    dn.tick_y(1)
     phase("n_fin")
     norms.finish(0)
     norms.finish(1)
-    phase("g_fin")
-    for s in range(0, HALF + 1):
+    for s in range(0, 7):
         gu.finish(s)
-
-    def up_step(j):
-        w = jnp.concatenate(
-            [wgu[:, :, j * 128 : (j + 1) * 128].reshape(D, 128),
-             wgu[:, :, 640 + j * 128 : 768 + j * 128].reshape(D, 128)], axis=1
-        )
-        v = dot(nf[...].reshape(TOK, D), w)
-        g = v[:, 0:128]
-        hid[:, j * 128 : (j + 1) * 128] = (g / (1.0 + jnp.exp(-g)) * v[:, 128:256]).astype(BF16)
-
-    phase("up0")
-    up_step(0)
-    up_step(1)
+    phase("early0")
+    up_early(0)
+    up_early(1)
+    phase("a8")
+    gu.tick_a(8, 0)
+    gu.tick_y(8)
+    gu.tick_a(8, 1)
+    dn.tick_a(4, 0)
+    dn.tick_a(4, 1)
+    dn.tick_b(5)
+    dn.tick_y(2)
+    phase("early1")
+    up_early(2)
+    up_early(3)
     phase("d5")
-    dn.tick_b(6)
-    dn.tick_y(4)
     dn.tick_a(5, 0)
     dn.tick_a(5, 1)
-    dn.tick_y(5)
-    phase("up1")
-    up_step(2)
-    up_step(3)
+    dn.tick_b(6)
+    dn.tick_y(3)
+    phase("early2")
+    up_early(4)
+    acc[:, 1280:1408] = up_dot(0, EARLY, 1280)
+    phase("g_fin")
+    for s in range(7, HALF + 1):
+        gu.finish(s)
+
+    phase("up0")
+    for j in range(4):
+        up_step(j)
     phase("d6")
-    dn.tick_b(7)
     dn.tick_a(6, 0)
     dn.tick_a(6, 1)
-    dn.tick_y(6)
+    dn.tick_b(7)
+    dn.tick_y(4)
     phase("up2")
     up_step(4)
-    v = dot(nf[...].reshape(TOK, D), wgu[:, :, 1280:1408].reshape(D, 128))
+    v = acc[:, 1280:1408] + up_dot(EARLY, NZ, 1280)
     v = v / (1.0 + jnp.exp(-v)) * pltpu.roll(v, 64, 1)
     low = lax.broadcasted_iota(jnp.int32, (TOK, 128), 1) < 64
     hid[:, 640:768] = jnp.where(low, v, 0.0).astype(BF16)
@@ -665,17 +694,29 @@
         mine = part[xb * 2 + net.c, :, span(k)].astype(F32)
         return mine + pr[xb, :, span(k)].astype(F32)
 
+    def hop(k, i, value, to):
+        ps[i, :, span(k)] = value.astype(BF16)
+        send(ps.at[i, :, span(k)], rs.at[i, :, span(k)],
+             r_send.at[3 * k + i], r_recv.at[3 * k + i], tp=to)
+
+    def landed(k, i, frm):
+        arrived(rs.at[i, :, span(k)], r_send.at[0], r_recv.at[3 * k + i], tp=frm)
+        return rs[i, :, span(k)].astype(F32)
+
     def sum_pair(k):
-        for i, (xb, to) in enumerate(((net.x2, net.tp2), (net.xm, net.tpm), (net.xp, net.tpp))):
-            ps[i, :, span(k)] = pair(k, xb).astype(BF16)
-            send(ps.at[i, :, span(k)], rs.at[i, :, span(k)],
-                 r_send.at[3 * k + i], r_recv.at[3 * k + i], tp=to)
+        hop(k, 0, pair(k, net.x2), net.tp2 if k == NC - 1 else net.tpp)
+        hop(k, 1, pair(k, net.xm), net.tpm)
+        if k == NC - 1:
+            hop(k, 2, pair(k, net.xp), net.tpp)
+
+    def sum_relay(k):
+        near = pair(k, net.xp)
+        hop(k, 2, near + landed(k, 0, net.tpm), net.tpp)
 
     def sum_finish(k):
-        total = pair(k, net.x)
-        for i, frm in enumerate((net.tp2, net.tpp, net.tpm)):
-            arrived(rs.at[i, :, span(k)], r_send.at[0], r_recv.at[3 * k + i], tp=frm)
-            total = total + rs[i, :, span(k)].astype(F32)
+        total = pair(k, net.x) + landed(k, 1, net.tpp) + landed(k, 2, net.tpm)
+        if k == NC - 1:
+            total = total + landed(k, 0, net.tp2)
         total = total.astype(BF16).astype(F32)
         for i in range(2 * (SPANS[k][1] - SPANS[k][0])):
             cols = pl.ds(pl.multiple_of(place(2 * SPANS[k][0] + i) * 128, 128), 128)
@@ -683,54 +724,70 @@
             out_ref[:, cols] = v.astype(BF16)
 
     phase("w0")
-    dn.tick_b(8)
     dn.finish(1)
     down_step(0)
     dn.finish(2)
     down_step(1)
-    phase("d7")
-    dn.tick_a(7, 0)
-    dn.tick_a(7, 1)
-    dn.tick_y(7)
-    dn.tick_y(8)
+    sum_start(0)
     phase("w2")
     dn.finish(3)
     down_step(2)
-    sum_start(0)
+    sum_pair(0)
+    phase("d7")
+    dn.tick_y(5)
+    dn.tick_a(7, 0)
+    dn.tick_a(7, 1)
+    dn.tick_b(8)
+    dn.tick_y(6)
+    phase("w3")
     dn.finish(4)
     down_step(3)
+    sum_start(1)
+    phase("d8")
+    dn.tick_y(7)
+    dn.tick_a(8, 0)
+    dn.tick_a(8, 1)
+    dn.tick_y(8)
     phase("w4")
-    sum_pair(0)
+    sum_relay(0)
+    sum_pair(1)
+    phase("w4d")
     dn.finish(5)
     down_step(4)
-    phase("w5")
     dn.finish(6)
     down_step(5)
-    sum_start(1)
+    sum_start(2)
     phase("w6")
     dn.finish(7)
     down_step(6)
-    sum_start(2)
-    sum_pair(1)
-    phase("d8")
-    dn.tick_a(8, 0)
-    dn.tick_a(8, 1)
+    phase("w7")
     dn.finish(0)
     dn.finish(8)
-    phase("w7")
     down_step(7)
     sum_start(3)
-    phase("rs")
+    phase("pair2")
+    sum_pair(2)
+    sum_relay(1)
+    phase("pair3")
+    sum_pair(3)
     sum_finish(0)
-    sum_pair(2)
-    sum_pair(3)
+    phase("relay2")
+    sum_relay(2)
     sum_finish(1)
+    phase("rs2")
     sum_finish(2)
+    phase("rs3")
     sum_finish(3)
 
     phase("drain")
     for cp in net.sent:
         cp.wait_send()
+    for k in range(1, NZ):
+
+        @pl.when(z + k < NZ)
+        def _():
+            net.copy(tb.at[z], tb.at[z], t_send.at[k], t_recv.at[z], sp_0=(z + k) % NZ).wait_send()
+
     phase(None)
 
 
@@ -763,6 +820,7 @@
         vmem((64, FL), F32),
         vmem((64, FL), F32),
         vmem((ROWS, D), F32),
+        vmem((TOK, GU), F32),
     ]
     counts = RING_SEMS + RING_SEMS + [
         2 * NT, 14, 2 * NT, 14, NY, NY, NZ, NZ, NT, NT, NC * NX, NC * 4, NC * 3, NC * 3,

time: 102 us -> 99.5 us (0.975)
  Pallas kernels: 99.8 us -> 97.7 us
    pallas_call x1, Pallas kernels: 99.8 us -> 97.7 us  [on_device(): pl.pallas_call(kernel, out_shape=jax.ShapeDtypeStruct((ROWS, D), BF16), i...]
where the time goes in v3:
time: 99.5 us; the launch traced here: 99.3 us
  Pallas kernels  97.7 us (98%)
  local copies, waits for them, and re-layouts  1.67 us (2%)
    pallas_call x1, Pallas kernels, on_device(): pl.pallas_call(kernel, out_shape=jax.ShapeDtypeStruct((ROWS, D), BF16), i...  97.7 us

profile of v3, /device:TPU:1, one launch (start us, length us, event | category | flops | bytes accessed | tf_op | source)
XLA Modules:
  0.0 99.3 jit_solution(16398967692088469284)
XLA Ops:
  0.0 97.7 %shard_map.145 = bf16[64,2048]{1,0:T(8,128)(2,1)} custom-call(bf16[512,128]{1,0:T(8,128)(2,1)} %x_ref.1, f32[8,64]{1,0:T(8,128)} %dr_ref.1, f32[8,64]{1,0:T(8,128)} %di_ref.1, f32[1,8]{1,0:T(1,128)} %bitcast.18, f32[128,64]{1,0:T(8,128)} %bitcast.12, f32[128,64]{1,0:T(8,128)} %bitcast.13, f32[128,64]{1,0:T(8,128)} %bitcast.14, f32[128,64]{1,0:T(8,128)} %bitcast.15, ...), custom_call_target="tpu_custom_call" | custom-call | tf_op jit(solution)/shard_map/pallas_call | solution.py:829
  97.7 1.7 %copy.17 = bf16[64,2048]{1,0:T(8,128)(2,1)} copy(bf16[64,2048]{1,0:T(8,128)(2,1)} %shard_map.145) | data formatting | bytes 524288

commit v4 on v3

--- a/solution.py
+++ b/solution.py
@@ -30,6 +30,7 @@
 CA = 512
 SPANS = ((0, 2), (2, 4), (4, 6), (6, 8))
 NC = len(SPANS)
+STRAIGHT = 1
 
 
 def discrete(decay_real, decay_imag, log_step):
@@ -276,8 +277,10 @@
 
 
 def kernel(
-    x_ref, dr_ref, di_ref, ls_ref, inr_ref, ini_ref, our_ref, oui_ref, skip_ref, op_ref, gain_ref,
-    res_ref, wg_ref, wu_ref, wd_ref, out_ref,
+    x_in, dr_in, di_in, ls_in, inr_in, ini_in, our_in, oui_in, skip_in, op_in, gain_in,
+    res_in, wg_in, wu_in, wd_in, keep_ref, out_ref,
+    x_ref, dr_ref, di_ref, ls_ref, inr_ref, ini_ref, our_ref, oui_ref, skip_ref, gain_ref,
+    res_ref, wg_ref, wu_ref, wd_ref,
     wgu, wdn, opall, sb, tb, act, acts, nf, hid, part, pr, ps, rs,
     ur, ui, mr, mi, er, ei, pcr, pci, carried, acc, *sems,
 ):
@@ -288,7 +291,16 @@
     gu = Ring(net, wgu, sems[0:8])
     dn = Ring(net, wdn, sems[8:16])
     (o_recv, o_send, n_recv, n_send, s_recv, s_send, t_recv, t_send, a_recv, a_send,
-     p_recv, p_send, r_recv, r_send) = sems[16:]
+     p_recv, p_send, r_recv, r_send, in_sem) = sems[16:]
+    pulls = [
+        pltpu.make_async_copy(src, dst, in_sem.at[i])
+        for i, (src, dst) in enumerate((
+            (wg_in, wg_ref), (wu_in, wu_ref), (wd_in, wd_ref), (op_in, opall.at[t]),
+            (dr_in, dr_ref), (di_in, di_ref), (ls_in, ls_ref), (x_in, x_ref),
+            (inr_in, inr_ref), (ini_in, ini_ref), (our_in, our_ref), (oui_in, oui_ref),
+            (skip_in, skip_ref), (gain_in, gain_ref), (res_in, res_ref),
+        ))
+    ]
     oproj = Pool(net, opall, o_recv, o_send)
     norms = Pool(net, nf, n_recv, n_send)
 
@@ -302,6 +314,10 @@
         pl.semaphore_signal(barrier, inc=1, device_id={"tp": (t + k) % NT}, device_id_type=MESH)
 
     phase("own")
+    for pull in pulls:
+        pull.start()
+    for pull in pulls[:3]:
+        pull.wait()
     own = z * NY + y
     wgu[own, :, 0:640] = wg_ref[:, 0:640]
     wgu[own, :, 640:1280] = wu_ref[:, 0:640]
@@ -309,9 +325,21 @@
     wdn[own, :, 0:640] = wd_ref[0:16, 0:640]
     wdn[own, :, 640:1280] = wd_ref[16:32, 0:640]
     wdn[own, :, 1280:1408] = jnp.concatenate([wd_ref[0:16, 640:704], wd_ref[16:32, 640:704]], axis=1)
-    opall[t] = op_ref[...]
+    pulls[3].wait()
+
+    phase("barrier")
+    pl.semaphore_wait(barrier, NT - 1 + NY - 1 + NZ - 1)
+
+    phase("first_sends")
+    gu.own_bz()
+    gu.start_ya()
+    oproj.start(0)
+    oproj.start(1)
+    gu.own_by()
 
     phase("coef")
+    for pull in pulls[4:]:
+        pull.wait()
     eight = lax.broadcasted_iota(jnp.int32, (8, 8), 0) == lax.broadcasted_iota(jnp.int32, (8, 8), 1)
     log_step = jnp.sum(
         jnp.where(eight, jnp.broadcast_to(ls_ref[...], (8, 8)), 0.0), axis=1, keepdims=True
@@ -383,6 +411,9 @@
     last = (e[0][63:64], e[1][63:64])
     sb[y, 0:4, :] = packed(last[0])
     sb[y, 4:8, :] = packed(last[1])
+    for k in range(1, NY):
+        send(sb.at[y], sb.at[y], s_send.at[k], s_recv.at[y], sp_1=(y + k) % NY)
+
     phase("lead")
     lead = (jnp.ones((64, FL), F32), jnp.zeros((64, FL), F32))
     for b, q in enumerate(ladder):
@@ -398,20 +429,15 @@
         mr[k] = jnp.where(block, dot(hi, spread), 0.0).astype(BF16)
         mi[k] = jnp.where(block, dot(lo, spread), 0.0).astype(BF16)
 
-    phase("barrier")
-    pl.semaphore_wait(barrier, NT - 1 + NY - 1 + NZ - 1)
-
-    phase("first_sends")
-    for k in range(1, NY):
-        send(sb.at[y], sb.at[y], s_send.at[k], s_recv.at[y], sp_1=(y + k) % NY)
-    gu.own_bz()
-    gu.start_ya()
-    oproj.start(0)
-    oproj.start(1)
-    gu.own_by()
-
     phase("b1")
     gu.tick_b(1)
+    phase("own_a")
+    gu.own_a()
+    dn.start_ya()
+    phase("b2")
+    gu.tick_b(2)
+    gu.tick_y(0)
+    dn.own_bz()
     phase("s_wait")
     for k in range(1, NY):
         yk = (y + k) % NY
@@ -439,11 +465,6 @@
             cp.start()
 
 
-    phase("own_a")
-    gu.own_a()
-    phase("b2")
-    gu.tick_b(2)
-    gu.tick_y(0)
     phase("a1")
     gu.tick_a(1, 0)
     phase("op0")
@@ -453,9 +474,12 @@
     phase("b3")
     gu.tick_b(3)
     gu.tick_y(1)
-
     phase("op1")
     oproj.forward(1)
+    phase("a2")
+    gu.tick_a(2, 0)
+    gu.tick_a(2, 1)
+    dn.own_a()
 
     phase("t_wait")
     for b in range(NZ - 1):
@@ -507,17 +531,13 @@
         send(act.at[tk], acts.at[t], a_send.at[k], a_recv.at[t], tp=tk)
     acts[t] = act[t]
 
-    phase("a2")
-    gu.tick_a(2, 0)
-    gu.tick_a(2, 1)
     phase("b4")
     gu.tick_b(4)
     phase("y2")
     gu.tick_y(2)
-    dn.start_ya()
+    dn.tick_b(1)
     phase("a3")
     gu.tick_a(3, 0)
-    dn.own_bz()
     gu.tick_a(3, 1)
     phase("op_last")
     oproj.last(0)
@@ -525,6 +545,10 @@
     phase("b5")
     gu.tick_b(5)
     gu.tick_y(3)
+    phase("d1")
+    dn.tick_a(1, 0)
+    dn.tick_a(1, 1)
+    dn.own_by()
     phase("op_fin")
     oproj.finish(0)
     oproj.finish(1)
@@ -568,52 +592,54 @@
     squares = lax.fori_loop(0, D // 512, mix_step, jnp.zeros((ROWS, 1), F32))
     gu.tick_a(4, 0)
     gu.tick_a(4, 1)
-    dn.own_a()
+    dn.tick_b(2)
     squares = lax.fori_loop(D // 512, D // 256, mix_step, squares)
     scale = lax.rsqrt(squares * (1.0 / D) + 1e-06)
     for o in range(NZ):
         src = pl.ds(pl.multiple_of(near(o) * 128, 128), 128)
         nf[t, :, o * 128 : (o + 1) * 128] = (carried[:, src] * scale * gain_ref[:, src]).astype(BF16)
+    keep = pltpu.make_async_copy(carried, keep_ref, in_sem.at[15])
     norms.start(0)
     norms.start(1)
+    keep.start()
     phase("b6")
     gu.tick_b(6)
     gu.tick_y(4)
-    dn.tick_b(1)
-    dn.own_by()
     phase("a5")
     gu.tick_a(5, 0)
+    dn.tick_a(2, 0)
     gu.tick_a(5, 1)
-    dn.tick_a(1, 0)
+    dn.tick_a(2, 1)
     phase("n0")
     norms.forward(0)
     phase("b7")
-    dn.tick_a(1, 1)
     gu.tick_b(7)
     gu.tick_y(5)
-    dn.tick_b(2)
+    dn.tick_b(3)
+    dn.tick_y(0)
     phase("n1")
     norms.forward(1)
     phase("a6")
     gu.tick_a(6, 0)
-    dn.tick_a(2, 0)
+    dn.tick_a(3, 0)
     gu.tick_a(6, 1)
-    dn.tick_a(2, 1)
+    dn.tick_a(3, 1)
     norms.last(0)
     phase("b8")
     gu.tick_b(8)
     gu.tick_y(6)
-    dn.tick_b(3)
-    dn.tick_y(0)
+    dn.tick_b(4)
+    dn.tick_y(1)
     norms.last(1)
     phase("a7")
     gu.tick_a(7, 0)
-    dn.tick_a(3, 0)
+    dn.tick_a(4, 0)
     gu.tick_a(7, 1)
-    dn.tick_a(3, 1)
+    dn.tick_a(4, 1)
     gu.tick_y(7)
-    dn.tick_b(4)
-    dn.tick_y(1)
+    dn.tick_b(5)
+    dn.tick_y(2)
+    gu.tick_y(8)
     phase("n_fin")
     norms.finish(0)
     norms.finish(1)
@@ -624,21 +650,16 @@
     up_early(1)
     phase("a8")
     gu.tick_a(8, 0)
-    gu.tick_y(8)
-    gu.tick_a(8, 1)
-    dn.tick_a(4, 0)
-    dn.tick_a(4, 1)
-    dn.tick_b(5)
-    dn.tick_y(2)
+    dn.tick_a(5, 0)
     phase("early1")
     up_early(2)
-    up_early(3)
-    phase("d5")
-    dn.tick_a(5, 0)
+    phase("a8b")
+    gu.tick_a(8, 1)
     dn.tick_a(5, 1)
     dn.tick_b(6)
     dn.tick_y(3)
     phase("early2")
+    up_early(3)
     up_early(4)
     acc[:, 1280:1408] = up_dot(0, EARLY, 1280)
     phase("g_fin")
@@ -704,24 +725,25 @@
         return rs[i, :, span(k)].astype(F32)
 
     def sum_pair(k):
-        hop(k, 0, pair(k, net.x2), net.tp2 if k == NC - 1 else net.tpp)
+        hop(k, 0, pair(k, net.x2), net.tp2 if k >= STRAIGHT else net.tpp)
         hop(k, 1, pair(k, net.xm), net.tpm)
-        if k == NC - 1:
+        if k >= STRAIGHT:
             hop(k, 2, pair(k, net.xp), net.tpp)
 
     def sum_relay(k):
+        if k >= STRAIGHT:
+            return
         near = pair(k, net.xp)
         hop(k, 2, near + landed(k, 0, net.tpm), net.tpp)
 
     def sum_finish(k):
         total = pair(k, net.x) + landed(k, 1, net.tpp) + landed(k, 2, net.tpm)
-        if k == NC - 1:
+        if k >= STRAIGHT:
             total = total + landed(k, 0, net.tp2)
-        total = total.astype(BF16).astype(F32)
+        total = total.astype(BF16)
         for i in range(2 * (SPANS[k][1] - SPANS[k][0])):
             cols = pl.ds(pl.multiple_of(place(2 * SPANS[k][0] + i) * 128, 128), 128)
-            v = carried[:, cols] + 0.5 * total[:, i * 128 : (i + 1) * 128]
-            out_ref[:, cols] = v.astype(BF16)
+            out_ref[:, cols] = total[:, i * 128 : (i + 1) * 128]
 
     phase("w0")
     dn.finish(1)
@@ -729,50 +751,49 @@
     dn.finish(2)
     down_step(1)
     sum_start(0)
+    phase("d7")
+    dn.tick_a(7, 0)
+    dn.tick_a(7, 1)
+    dn.tick_b(8)
+    dn.tick_y(5)
+    dn.tick_y(6)
     phase("w2")
     dn.finish(3)
     down_step(2)
     sum_pair(0)
-    phase("d7")
-    dn.tick_y(5)
-    dn.tick_a(7, 0)
-    dn.tick_a(7, 1)
-    dn.tick_b(8)
-    dn.tick_y(6)
-    phase("w3")
     dn.finish(4)
     down_step(3)
     sum_start(1)
     phase("d8")
-    dn.tick_y(7)
     dn.tick_a(8, 0)
     dn.tick_a(8, 1)
+    dn.tick_y(7)
     dn.tick_y(8)
     phase("w4")
-    sum_relay(0)
-    sum_pair(1)
-    phase("w4d")
     dn.finish(5)
     down_step(4)
+    sum_pair(1)
+    phase("w5")
     dn.finish(6)
     down_step(5)
     sum_start(2)
+    sum_relay(0)
     phase("w6")
     dn.finish(7)
     down_step(6)
+    sum_pair(2)
     phase("w7")
     dn.finish(0)
     dn.finish(8)
     down_step(7)
     sum_start(3)
-    phase("pair2")
-    sum_pair(2)
+    phase("relay1")
     sum_relay(1)
-    phase("pair3")
     sum_pair(3)
+    phase("rs0")
+    sum_relay(2)
     sum_finish(0)
-    phase("relay2")
-    sum_relay(2)
+    phase("rs1")
     sum_finish(1)
     phase("rs2")
     sum_finish(2)
@@ -780,6 +801,7 @@
     sum_finish(3)
 
     phase("drain")
+    keep.wait()
     for cp in net.sent:
         cp.wait_send()
     for k in range(1, NZ):
@@ -798,6 +820,20 @@
     vmem = pltpu.VMEM
     dma = pltpu.SemaphoreType.DMA
     scratch = [
+        vmem((TOK, CHD), BF16),
+        vmem((8, 64), F32),
+        vmem((8, 64), F32),
+        vmem((1, 8), F32),
+        vmem((CHD, 64), F32),
+        vmem((CHD, 64), F32),
+        vmem((CHD, 64), F32),
+        vmem((CHD, 64), F32),
+        vmem((1, CHD), F32),
+        vmem((1, D), F32),
+        vmem((ROWS, D), BF16),
+        vmem((32, FFD), BF16),
+        vmem((32, FFD), BF16),
+        vmem((32, FFD), BF16),
         vmem((NZ * NY, 32, GU), BF16),
         vmem((NZ * NY, 16, GU), BF16),
         vmem((NT, CHD, D), BF16),
@@ -823,14 +859,14 @@
         vmem((TOK, GU), F32),
     ]
     counts = RING_SEMS + RING_SEMS + [
-        2 * NT, 14, 2 * NT, 14, NY, NY, NZ, NZ, NT, NT, NC * NX, NC * 4, NC * 3, NC * 3,
+        2 * NT, 14, 2 * NT, 14, NY, NY, NZ, NZ, NT, NT, NC * NX, NC * 4, NC * 3, NC * 3, 16,
     ]
     scratch += [dma((n,)) for n in counts]
-    return pl.pallas_call(
+    carried, down = pl.pallas_call(
         kernel,
-        out_shape=jax.ShapeDtypeStruct((ROWS, D), BF16),
-        in_specs=[pl.BlockSpec(memory_space=vmem)] * 15,
-        out_specs=pl.BlockSpec(memory_space=vmem),
+        out_shape=(jax.ShapeDtypeStruct((ROWS, D), F32), jax.ShapeDtypeStruct((ROWS, D), BF16)),
+        in_specs=[pl.BlockSpec(memory_space=pl.ANY)] * 15,
+        out_specs=(pl.BlockSpec(memory_space=pl.ANY), pl.BlockSpec(memory_space=vmem)),
         scratch_shapes=scratch,
         compiler_params=pltpu.CompilerParams(
             collective_id=0, has_side_effects=True, vmem_limit_bytes=60 * 1024 * 1024
@@ -843,6 +879,7 @@
         skip.reshape(1, CHD), out_proj, norm_gain.reshape(1, D),
         residual, w_gate, w_up, w_down.T,
     )
+    return (carried + 0.5 * down.astype(F32)).astype(BF16)
 
 
 def solution(mesh):

time: 99.5 us -> 96.9 us (0.974)
  Pallas kernels: 97.7 us -> 94.9 us
  other arithmetic: 0 us -> 1.88 us
  local copies, waits for them, and re-layouts: 1.67 us -> 0 us
    pallas_call x1, Pallas kernels: 97.7 us -> 94.9 us  [on_device(): pl.pallas_call(kernel, out_shape=(jax.ShapeDtypeStruct((ROWS, D), F32), j...]
    convert_element_type x0 -> x1, other arithmetic: none -> 1.88 us  [on_device(): return (carried + 0.5 * down.astype(F32)).astype(BF16)]
    unnamed x1 -> x0, local copies, waits for them, and re-layouts: 1.67 us -> none
where the time goes in v4:
time: 96.9 us; the launch traced here: 96.8 us
  Pallas kernels  94.9 us (98%)
  other arithmetic  1.88 us (2%)
    pallas_call x1, Pallas kernels, on_device(): pl.pallas_call(kernel, out_shape=(jax.ShapeDtypeStruct((ROWS, D), F32), j...  94.9 us

profile of v4, /device:TPU:1, one launch (start us, length us, event | category | flops | bytes accessed | tf_op | source)
XLA Modules:
  0.0 96.8 jit_solution(16872764964021586236)
XLA Ops:
  0.0 94.9 %shard_map.145 = (f32[64,2048]{1,0:T(8,128)}, bf16[64,2048]{1,0:T(8,128)(2,1)}) custom-call(bf16[512,128]{1,0:T(8,128)(2,1)} %x_in.1, f32[8,64]{1,0:T(8,128)} %dr_in.1, f32[8,64]{1,0:T(8,128)} %di_in.1, f32[1,8]{1,0:T(1,128)} %bitcast.18, f32[128,64]{1,0:T(8,128)} %bitcast.12, f32[128,64]{1,0:T(8,128)} %bitcast.13, f32[128,64]{1,0:T(8,128)} %bitcast.14, ...), custom_call_target="tpu_custom_call" | custom-call | tf_op jit(solution)/shard_map/pallas_call | solution.py:865
  94.9 1.9 %add_convert_fusion = bf16[64,2048]{1,0:T(8,128)(2,1)} fusion(f32[64,2048]{1,0:T(8,128)} %get-tuple-element.7, bf16[64,2048]{1,0:T(8,128)(2,1)} %get-tuple-element.8), kind=kLoop, calls=%fused_computation | loop fusion | flops 524288 | bytes 1048576 | tf_op jit(solution)/shard_map/convert_element_type | solution.py:882

commit v5 on v4

--- a/solution.py
+++ b/solution.py
@@ -28,9 +28,10 @@
 FFD = 704
 GU = 2 * FFD
 CA = 512
+CD = 384
 SPANS = ((0, 2), (2, 4), (4, 6), (6, 8))
 NC = len(SPANS)
-STRAIGHT = 1
+STRAIGHT = 2
 
 
 def discrete(decay_real, decay_imag, log_step):
@@ -91,19 +92,19 @@
 class Ring:
     count = 33
 
-    def __init__(self, net, buf, sems):
-        self.net, self.buf = net, buf
+    def __init__(self, net, buf, ca, sems):
+        self.net, self.buf, self.ca = net, buf, ca
         (self.ya_recv, self.ya_send, self.za_recv, self.za_send,
          self.zb_recv, self.zb_send, self.yb_recv, self.yb_send) = sems
 
     def a_y(self, zb, yb):
-        return self.buf.at[zb * NY + yb, :, 0:CA]
+        return self.buf.at[zb * NY + yb, :, 0 : self.ca]
 
     def a_z(self, zb, h):
-        return self.buf.at[pl.ds(zb * NY + 2 * h, 2), :, 0:CA]
+        return self.buf.at[pl.ds(zb * NY + 2 * h, 2), :, 0 : self.ca]
 
     def b(self, zb, yb):
-        return self.buf.at[zb * NY + yb, :, CA:GU]
+        return self.buf.at[zb * NY + yb, :, self.ca : GU]
 
     def start_ya(self):
         n = self.net
@@ -157,14 +158,20 @@
             if n.goes_on(chain, s):
                 self.forward_a(zb, chain, s, h)
 
-    def tick_b(self, s):
+    def start_y(self, s):
+        n = self.net
+        for chain in n.chains(s):
+            self.start_yb(n.block(chain, s), n.order(chain, s))
+
+    def tick_b(self, s, along_y=True):
         n = self.net
         for chain in n.chains(s):
             zb = n.block(chain, s)
             n.arrived(self.b(zb, n.y), self.zb_send.at[0], self.zb_recv.at[zb], sp_0=n.zm)
             if n.goes_on(chain, s):
                 self.forward_b(zb, chain, s)
-            self.start_yb(zb, n.order(chain, s))
+            if along_y:
+                self.start_yb(zb, n.order(chain, s))
 
     def tick_y(self, s):
         n = self.net
@@ -288,8 +295,8 @@
     phase = Phase()
     z, y, t = net.z, net.y, net.t
     send, arrived = net.send, net.arrived
-    gu = Ring(net, wgu, sems[0:8])
-    dn = Ring(net, wdn, sems[8:16])
+    gu = Ring(net, wgu, CA, sems[0:8])
+    dn = Ring(net, wdn, CD, sems[8:16])
     (o_recv, o_send, n_recv, n_send, s_recv, s_send, t_recv, t_send, a_recv, a_send,
      p_recv, p_send, r_recv, r_send, in_sem) = sems[16:]
     pulls = [
@@ -628,18 +635,19 @@
     phase("b8")
     gu.tick_b(8)
     gu.tick_y(6)
-    dn.tick_b(4)
-    dn.tick_y(1)
+    dn.tick_b(4, along_y=False)
     norms.last(1)
     phase("a7")
     gu.tick_a(7, 0)
     dn.tick_a(4, 0)
+    gu.tick_y(7)
     gu.tick_a(7, 1)
     dn.tick_a(4, 1)
-    gu.tick_y(7)
+    gu.tick_y(8)
+    dn.start_y(4)
+    dn.tick_y(1)
     dn.tick_b(5)
     dn.tick_y(2)
-    gu.tick_y(8)
     phase("n_fin")
     norms.finish(0)
     norms.finish(1)
@@ -653,15 +661,15 @@
     dn.tick_a(5, 0)
     phase("early1")
     up_early(2)
+    phase("early2")
+    up_early(3)
+    up_early(4)
+    acc[:, 1280:1408] = up_dot(0, EARLY, 1280)
     phase("a8b")
     gu.tick_a(8, 1)
     dn.tick_a(5, 1)
     dn.tick_b(6)
     dn.tick_y(3)
-    phase("early2")
-    up_early(3)
-    up_early(4)
-    acc[:, 1280:1408] = up_dot(0, EARLY, 1280)
     phase("g_fin")
     for s in range(7, HALF + 1):
         gu.finish(s)

time: 96.9 us -> 94.8 us (0.978)
  Pallas kernels: 94.9 us -> 92.7 us
    pallas_call x1, Pallas kernels: 94.9 us -> 92.7 us  [on_device(): pl.pallas_call(kernel, out_shape=(jax.ShapeDtypeStruct((ROWS, D), F32), j...]
where the time goes in v5:
time: 94.8 us; the launch traced here: 94.6 us
  Pallas kernels  92.7 us (98%)
  other arithmetic  1.88 us (2%)
    pallas_call x1, Pallas kernels, on_device(): pl.pallas_call(kernel, out_shape=(jax.ShapeDtypeStruct((ROWS, D), F32), j...  92.7 us

profile of v5, /device:TPU:1, one launch (start us, length us, event | category | flops | bytes accessed | tf_op | source)
XLA Modules:
  0.0 94.6 jit_solution(8252861299270542248)
XLA Ops:
  0.0 92.7 %shard_map.145 = (f32[64,2048]{1,0:T(8,128)}, bf16[64,2048]{1,0:T(8,128)(2,1)}) custom-call(bf16[512,128]{1,0:T(8,128)(2,1)} %x_in.1, f32[8,64]{1,0:T(8,128)} %dr_in.1, f32[8,64]{1,0:T(8,128)} %di_in.1, f32[1,8]{1,0:T(1,128)} %bitcast.18, f32[128,64]{1,0:T(8,128)} %bitcast.12, f32[128,64]{1,0:T(8,128)} %bitcast.13, f32[128,64]{1,0:T(8,128)} %bitcast.14, ...), custom_call_target="tpu_custom_call" | custom-call | tf_op jit(solution)/shard_map/pallas_call | solution.py:873
  92.7 1.9 %add_convert_fusion = bf16[64,2048]{1,0:T(8,128)(2,1)} fusion(f32[64,2048]{1,0:T(8,128)} %get-tuple-element.7, bf16[64,2048]{1,0:T(8,128)(2,1)} %get-tuple-element.8), kind=kLoop, calls=%fused_computation | loop fusion | flops 524288 | bytes 1048576 | tf_op jit(solution)/shard_map/convert_element_type | solution.py:890
